TPU v7x, 32 devices: a whole 2x2x4 slice. The times are simulated.
32 devices in a mesh: ep: 8 (over z, y), tp: 4 (over x, core).
Axes of the slice: x: 2, y: 2, z: 4, core: 2. Of those that a mesh axis runs over, the one named last changes fastest.
Arguments:
- state_probe_logits: bfloat16 [8192, 1024], P('ep', 'tp'), may hold values from -6 to 6
- retention_logits: bfloat16 [8192, 1024], P('ep', 'tp'), may hold values from -12 to 12
- state_source_entries: bfloat16 [8192, 1024], P('ep', 'tp'), may hold values from -6 to 6
- state_result_switch_logits: bfloat16 [8192, 1024], P('ep', 'tp'), may hold values from -6 to 6
- retention_bound_margin: float32 [1024], P('tp'), may hold values from 0 to 0.07
- extra_fading_amount: float32 [8192, 8], P('ep', 'tp'), may hold values from -0.7 to 0
- state_result_scale: float32 [1024], P('tp'), may hold values from 0.1 to 1.9
- state_result_matrix: bfloat16 [1024, 2048], P(None, 'tp'), may hold values from -0.1875 to 0.1875
- second_slice_tokens: bfloat16 [4096, 2048], P('ep'), may hold values from -6 to 6
- specialist_assignment: int32 [4096, 2], P('ep'), may hold values from 0 to 7, all different within a row; in each aligned block of 128 rows (0 to 127, 128 to 255, ...) at most 64 rows name the same one
- selected_specialist_share: float32 [4096, 2], P('ep'), may hold values from 0.1 to 1
- leading_scale_vector: float32 [2048], replicated, may hold values from 0.1 to 1.9
- trailing_scale_vector: float32 [2048], replicated, may hold values from 0.1 to 1.9
- specialist_switch_matrix: bfloat16 [8, 2048, 2048], P('ep', None, 'tp'), may hold values from -0.3125 to 0.3125
- specialist_widen_matrix: bfloat16 [8, 2048, 2048], P('ep', None, 'tp'), may hold values from -0.3125 to 0.3125
- specialist_contract_matrix: bfloat16 [8, 2048, 2048], P('ep', 'tp'), may hold values from -0.125 to 0.125
Outputs:
- mixer_out: bfloat16 [8192, 2048], P('ep', 'tp')
- moe_out: bfloat16 [4096, 2048], P(('ep', 'tp'))
Inputs may be any that keep to these rules, and one draw needn't show every extreme that they name: `specialist_assignment`: each row names 2 different experts. In each aligned block of 128 rows no expert is named by more than 64 rows, a bound that some block reaches.
All inputs are finite; a program needn't handle non-finite values.
Results may differ from a plain program's by a relative error of at most 0.012.
Values may be sent and summed in bfloat16 or wider, within the bound.
A program may use at most 128 MiB of HBM per device.

v0:
```python
import functools

import jax
import jax.numpy as jnp
from jax import lax
from jax.experimental import pallas as pl
from jax.experimental.pallas import tpu as pltpu
from jax.sharding import PartitionSpec as P

HEAD = 128
SPAN = 128
TOK_DEV = 128

NORM_EPS = 1e-06
SWISH_ALPHA = 1.702
CLAMP_LIMIT = 7.0
MESH = pl.DeviceIdType.MESH
VMEM = pltpu.VMEM
DMA = pltpu.SemaphoreType.DMA
NT = (((1,), (1,)), ((), ()))
TN = (((0,), (0,)), ((), ()))


def xor(a, b, n):
    total, bit = 0, 1
    while bit < n:
        total = total + ((a // bit + b // bit) % 2) * bit
        bit *= 2
    return total


def places():
    i, j = lax.axis_index("ep"), lax.axis_index("tp")
    mate = j + 1 - 2 * (j % 2)
    cross = (j + 2) % 4
    return i, j, mate, cross


def greet(n, i, j, mate, cross):
    barrier = pltpu.get_barrier_semaphore()

    def one(s, c):
        pl.semaphore_signal(barrier, inc=1, device_id=((i + s) % n, j), device_id_type=MESH)
        return c

    lax.fori_loop(1, n, one, 0)
    for t in (mate, cross):
        pl.semaphore_signal(barrier, inc=1, device_id=(i, t), device_id_type=MESH)
    pl.semaphore_wait(barrier, n + 1)


def remote(src, dst, send, recv, where):
    return pltpu.make_async_remote_copy(
        src_ref=src, dst_ref=dst, send_sem=send, recv_sem=recv, device_id=where, device_id_type=MESH
    )


def span_step(t, probe, ret, val, margin, extra, raw, qdec, state, running):
    rows = pl.ds(pl.multiple_of(t * SPAN, SPAN), SPAN)
    width = probe.shape[1]
    x = probe[rows, :].astype(jnp.float32)
    q = x * jax.nn.sigmoid(x) * HEAD ** (-0.5)
    k = margin[...] * jax.nn.sigmoid(-ret[rows, :].astype(jnp.float32))
    logs = jnp.log1p(-k)
    row = lax.broadcasted_iota(jnp.int32, (SPAN, SPAN), 0)
    col = lax.broadcasted_iota(jnp.int32, (SPAN, SPAN), 1)
    causal = row >= col
    tril = jnp.where(causal, 1.0, 0.0).astype(jnp.float32)
    for h in range(width // HEAD):
        cols = slice(h * HEAD, (h + 1) * HEAD)
        qh, kh = q[:, cols], k[:, cols]
        ld = logs[:, cols] + extra[rows, h : h + 1]
        cum = jnp.dot(
            tril, ld, precision=lax.Precision.HIGHEST, preferred_element_type=jnp.float32
        )
        middle = cum[SPAN // 2 - 1 : SPAN // 2, :]
        last = cum[SPAN - 1 :, :]
        a = (qh * jnp.exp(cum - middle)).astype(jnp.bfloat16)
        b = (kh * jnp.exp(middle - cum)).astype(jnp.bfloat16)
        qe = qh * jnp.exp(cum)
        kd = (kh * jnp.exp(last - cum)).astype(jnp.bfloat16)
        v = val[rows, cols]
        s = lax.dot_general(a, b, NT, preferred_element_type=jnp.float32)
        s = jnp.where(causal, s, 0.0).astype(jnp.bfloat16)
        st = state[h]
        out = jnp.dot(s, v, preferred_element_type=jnp.float32)
        out = out + lax.dot_general(
            qe.astype(jnp.bfloat16), st.astype(jnp.bfloat16), NT, preferred_element_type=jnp.float32
        )
        raw[rows, cols] = out
        before = running[0:1, cols]
        qdec[rows, cols] = (qe * jnp.exp(before)).astype(jnp.bfloat16)
        state[h] = jnp.exp(last) * st + lax.dot_general(
            v, kd, TN, preferred_element_type=jnp.float32
        )
        running[:, cols] = running[:, cols] + last


def moe_kernel(
    n, packed, probe, ret, val, margin, extra, gate_hbm, up_hbm, down_hbm,
    raw, qdec, state_out, running, back,
    state, rows, part, gate_w, up_w, down_w, acc, sendb, recvb, fin,
    asend, arecv, xsend, xrecv, csend, crecv, dsend, drecv, own_sem, weight_sem,
    esend0, erecv0, esend1, erecv1, bsend, brecv, rsend, rrecv,
):
    i, j, mate, cross = places()
    mate_cross = (mate + 2) % 4
    spans = probe.shape[0] // SPAN
    capacity, features = packed.shape[1], packed.shape[2]
    loads = [
        pltpu.make_async_copy(src, dst, weight_sem.at[w])
        for w, (src, dst) in enumerate(((gate_hbm, gate_w), (up_hbm, up_w), (down_hbm, down_w)))
    ]
    for load in loads:
        load.start()
    greet(n, i, j, mate, cross)

    def direct(s):
        k = xor(i, s, n)
        return remote(packed.at[k], rows.at[i, j], asend.at[s], arecv.at[s], (k, j))

    def over_x(src, s):
        k = xor(i, s, n)
        return remote(src, rows.at[k, j], xsend.at[s], xrecv.at[s], (i, cross))

    def over_c(src, s):
        k = xor(i, s, n)
        return remote(src, rows.at[k, j], csend.at[s], crecv.at[s], (i, mate))

    def over_d(s):
        k = xor(i, s, n)
        return remote(rows.at[k, cross], rows.at[k, cross], dsend.at[s], drecv.at[s], (i, mate))

    def to_mate(s, near):
        k = xor(i, s, n)
        if near:
            return remote(part.at[k, mate], acc.at[0, k], esend0.at[s], erecv0.at[s], (i, mate))
        return remote(
            part.at[k, mate_cross], acc.at[1, k], esend1.at[s], erecv1.at[s], (i, mate)
        )

    def to_cross(s):
        return remote(sendb.at[s], recvb.at[s], bsend.at[s], brecv.at[s], (i, cross))

    def home(s):
        k = xor(i, s, n)
        return remote(fin.at[s], back.at[i], rsend.at[s], rrecv.at[s], (k, j))

    def home_in(s):
        k = xor(i, s, n)
        return remote(fin.at[s], back.at[k], rsend.at[s], rrecv.at[s], (k, j))

    def start_direct(t, c):
        direct(n - 1 - t).start()
        return c

    direct(1).start()
    lax.fori_loop(0, n - 2, start_direct, 0)
    own = pltpu.make_async_copy(packed.at[i], rows.at[i, j], own_sem)
    own.start()
    over_x(packed.at[i], 0).start()
    over_c(packed.at[i], 0).start()
    state[...] = jnp.zeros_like(state)
    running[...] = jnp.zeros_like(running)

    def order(t):
        return ((t + n - 1) // n) * (1 + (n - t) % (n - 1))

    def span(t):
        span_step(t, probe, ret, val, margin, extra, raw, qdec, state, running)

    def serve(t):
        s = order(t)
        k = xor(i, s, n)
        direct(s).wait_recv()
        over_x(rows.at[k, j], s).start()
        over_c(rows.at[k, j], s).start()

    def work(t):
        s = order(t)
        k = xor(i, s, n)
        over_c(packed.at[i], s).wait_recv()
        over_d(s).wait_recv()
        x = rows[k].reshape(4 * capacity, features)
        gate = jnp.dot(x, gate_w[...], preferred_element_type=jnp.float32)
        upward = jnp.dot(x, up_w[...], preferred_element_type=jnp.float32)
        act = clamped_unit(gate, upward).astype(jnp.bfloat16)
        step = 512
        for f in range(0, features, step):
            y = jnp.dot(act, down_w[:, f : f + step], preferred_element_type=jnp.float32)
            part[k, :, :, f : f + step] = y.astype(jnp.bfloat16).reshape(4, capacity, step)
        to_mate(s, False).start()
        to_mate(s, True).start()

    def first_sum(t):
        s = order(t)
        k = xor(i, s, n)
        to_mate(s, False).wait()
        x = part[k, cross].astype(jnp.float32) + acc[1, k].astype(jnp.float32)
        sendb[s] = x.astype(jnp.bfloat16)
        to_cross(s).start()

    def total(s):
        k = xor(i, s, n)
        to_mate(s, True).wait()
        to_cross(s).wait()
        x = part[k, j].astype(jnp.float32) + acc[0, k].astype(jnp.float32)
        return (x + recvb[s].astype(jnp.float32)).astype(jnp.bfloat16)

    def pump(t, c):
        @pl.when(t < spans)
        def _():
            span(t)

        @pl.when(t + 1 < n)
        def _():
            serve(t + 1)

        @pl.when(t < n)
        def _():
            s = order(t)
            over_x(packed.at[i], s).wait_recv()
            over_d(s).start()

        @pl.when((t >= 1) & (t < n + 1))
        def _():
            work(t - 1)

        @pl.when((t >= 2) & (t < n + 2))
        def _():
            first_sum(t - 2)

        @pl.when((t >= 4) & (t < n + 3))
        def _():
            s = order(t - 3)
            fin[s] = total(s)
            home(s).start()

        return c

    own.wait()
    for load in loads:
        load.wait()
    lax.fori_loop(0, max(n + 3, spans), pump, 0)
    back[i] = total(0)

    def finish(s, c):
        over_x(packed.at[i], s).wait_send()
        over_c(packed.at[i], s).wait_send()
        over_d(s).wait_send()
        return c

    lax.fori_loop(0, n, finish, 0)

    def finish_direct(s, c):
        direct(s).wait_send()
        home(s).wait_send()
        home_in(s).wait_recv()
        return c

    lax.fori_loop(1, n, finish_direct, 0)
    for h in range(state.shape[0]):
        state_out[h] = state[h].astype(jnp.bfloat16)


def moe(n, packed, probe, ret, val, margin, extra, gate_w, up_w, down_w):
    length, width = probe.shape
    heads = width // HEAD
    vm = pl.BlockSpec(memory_space=VMEM)
    hbm = pl.BlockSpec(memory_space=pl.ANY)
    chunk = packed.shape[1:]
    bf = jnp.bfloat16
    return pl.pallas_call(
        functools.partial(moe_kernel, n),
        name="moe",
        out_shape=(
            jax.ShapeDtypeStruct((length, width), jnp.float32),
            jax.ShapeDtypeStruct((length, width), bf),
            jax.ShapeDtypeStruct((heads, HEAD, HEAD), bf),
            jax.ShapeDtypeStruct((8, width), jnp.float32),
            jax.ShapeDtypeStruct(packed.shape, bf),
        ),
        in_specs=[vm] * 6 + [hbm] * 3,
        out_specs=(vm,) * 5,
        scratch_shapes=[
            VMEM((heads, HEAD, HEAD), jnp.float32),
            VMEM((n, 4) + chunk, bf),
            VMEM((n, 4) + chunk, bf),
            VMEM(gate_w.shape, bf),
            VMEM(up_w.shape, bf),
            VMEM(down_w.shape, bf),
            VMEM((2, n) + chunk, bf),
            VMEM((n,) + chunk, bf),
            VMEM((n,) + chunk, bf),
            VMEM((n,) + chunk, bf),
        ]
        + [DMA((n,))] * 8
        + [DMA, DMA((3,))]
        + [DMA((n,))] * 8,
        compiler_params=pltpu.CompilerParams(
            collective_id=0, has_side_effects=True, vmem_limit_bytes=60 * 2**20
        ),
        cost_estimate=pl.CostEstimate(
            flops=10**10, bytes_accessed=200 * 10**6, transcendentals=10**6
        ),
    )(packed, probe, ret, val, margin, extra, gate_w, up_w, down_w)


def mixer_kernel(
    n, chunks, raw, qdec, switch, state, decay, scale, weight,
    out,
    states, decays, gath, enter, ssend, srecv, esend, erecv,
    xsend, xrecv, csend, crecv, dsend, drecv,
):
    i, j, mate, cross = places()
    rows, width = raw.shape
    part = rows // chunks
    heads = width // HEAD
    greet(n, i, j, mate, cross)

    def send_state(s):
        k = (i + s) % n
        return remote(state, states.at[i], ssend.at[s], srecv.at[s], (k, j))

    def send_decay(s):
        k = (i + s) % n
        return remote(decay, decays.at[i], esend.at[s], erecv.at[s], (k, j))

    def begin(s, c):
        send_state(s).start()
        send_decay(s).start()
        return c

    lax.fori_loop(1, n, begin, 0)

    def end(s, c):
        send_state(s).wait()
        send_decay(s).wait()
        return c

    lax.fori_loop(1, n, end, 0)
    enter[...] = jnp.zeros_like(enter)

    def join(p, c):
        @pl.when(p < i)
        def _():
            for h in range(heads):
                d = decays[p, 0:1, h * HEAD : (h + 1) * HEAD]
                enter[h] = jnp.exp(d) * enter[h] + states[p, h].astype(jnp.float32)

        return c

    lax.fori_loop(0, n, join, 0)

    def at(c):
        return pl.ds(pl.multiple_of(c * part, part), part)

    def over_x(c):
        here = gath.at[j, at(c)]
        return remote(here, here, xsend.at[c], xrecv.at[c], (i, cross))

    def over_c(c):
        here = gath.at[j, at(c)]
        return remote(here, here, csend.at[c], crecv.at[c], (i, mate))

    def over_d(c):
        here = gath.at[cross, at(c)]
        return remote(here, here, dsend.at[c], drecv.at[c], (i, mate))

    def final(c, carry):
        r = at(c)
        for h in range(heads):
            cols = slice(h * HEAD, (h + 1) * HEAD)
            x = raw[r, cols] + lax.dot_general(
                qdec[r, cols], enter[h].astype(jnp.bfloat16), NT,
                preferred_element_type=jnp.float32,
            )
            x = x * lax.rsqrt(jnp.mean(x * x, axis=-1, keepdims=True) + NORM_EPS)
            g = switch[r, cols].astype(jnp.float32)
            gath[j, r, cols] = (x * scale[:, cols] * (g * jax.nn.sigmoid(g))).astype(jnp.bfloat16)
        over_x(c).start()
        over_c(c).start()
        return carry

    lax.fori_loop(0, chunks, final, 0)

    def pass_on(c, carry):
        over_x(c).wait()
        over_d(c).start()
        return carry

    lax.fori_loop(0, chunks, pass_on, 0)

    def project(c, carry):
        over_c(c).wait()
        over_d(c).wait()
        r = at(c)
        acc = jnp.dot(gath[0, r, :], weight[0:width, :], preferred_element_type=jnp.float32)
        for p in range(1, 4):
            acc = acc + jnp.dot(
                gath[p, r, :], weight[p * width : (p + 1) * width, :],
                preferred_element_type=jnp.float32,
            )
        out[r, :] = acc.astype(jnp.bfloat16)
        return carry

    lax.fori_loop(0, chunks, project, 0)


def mixer(n, raw, qdec, switch, state, decay, scale, weight):
    rows, width = raw.shape
    heads = width // HEAD
    chunks = 4
    vm = pl.BlockSpec(memory_space=VMEM)
    return pl.pallas_call(
        functools.partial(mixer_kernel, n, chunks),
        name="mixer",
        out_shape=jax.ShapeDtypeStruct((rows, weight.shape[1]), jnp.bfloat16),
        in_specs=[vm] * 7,
        out_specs=vm,
        scratch_shapes=[
            VMEM((n, heads, HEAD, HEAD), jnp.bfloat16),
            VMEM((n, 8, width), jnp.float32),
            VMEM((4, rows, width), jnp.bfloat16),
            VMEM((heads, HEAD, HEAD), jnp.float32),
        ]
        + [DMA((n,))] * 4
        + [DMA((chunks,))] * 6,
        compiler_params=pltpu.CompilerParams(
            collective_id=1, has_side_effects=True, vmem_limit_bytes=48 * 2**20
        ),
        cost_estimate=pl.CostEstimate(
            flops=10**9, bytes_accessed=60 * 10**6, transcendentals=10**6
        ),
    )(raw, qdec, switch, state, decay, scale, weight)


def rms_scale(values, gain):
    return values * lax.rsqrt(jnp.mean(values * values, axis=-1, keepdims=True) + NORM_EPS) * gain


def clamped_unit(gate, upward):
    glued = jnp.minimum(gate, CLAMP_LIMIT)
    linear = jnp.clip(upward, -CLAMP_LIMIT, CLAMP_LIMIT)
    return glued * jax.nn.sigmoid(SWISH_ALPHA * glued) * (linear + 1.0)


def slot_hits(routes, experts, capacity):
    tokens, top = routes.shape
    ids = jnp.arange(experts, dtype=jnp.int32)
    onehot = (routes[:, :, None] == ids).astype(jnp.float32)
    named = jnp.sum(onehot, axis=1)
    earlier = jnp.tril(jnp.ones((tokens, tokens), jnp.float32), -1)
    ahead = jnp.dot(earlier, named, preferred_element_type=jnp.float32)
    rank = jnp.sum(onehot * ahead[:, None, :], axis=2).astype(jnp.int32)
    slots = routes * capacity + rank
    return slots[:, :, None] == jnp.arange(experts * capacity, dtype=jnp.int32)


def shards(
    state_probe_logits,
    retention_logits,
    state_source_entries,
    state_result_switch_logits,
    retention_bound_margin,
    extra_fading_amount,
    state_result_scale,
    state_result_matrix,
    second_slice_tokens,
    specialist_assignment,
    selected_specialist_share,
    leading_scale_vector,
    trailing_scale_vector,
    specialist_switch_matrix,
    specialist_widen_matrix,
    specialist_contract_matrix,
):
    n = lax.axis_size("ep")
    experts = specialist_switch_matrix.shape[0] * n
    top_count = specialist_assignment.shape[1]
    capacity = 2 * TOK_DEV * top_count // experts
    first = lax.axis_index("tp") * TOK_DEV
    own_route = lax.dynamic_slice_in_dim(specialist_assignment, first, TOK_DEV, 0)
    own_weight = lax.dynamic_slice_in_dim(selected_specialist_share, first, TOK_DEV, 0)
    own_rows = lax.dynamic_slice_in_dim(second_slice_tokens, first, TOK_DEV, 0)
    normed = rms_scale(own_rows.astype(jnp.float32), leading_scale_vector).astype(jnp.bfloat16)
    hits = slot_hits(own_route, experts, capacity)
    pick = jnp.any(hits, axis=1).astype(jnp.bfloat16)
    packed = lax.dot_general(pick, normed, TN, preferred_element_type=jnp.float32)
    packed = packed.astype(jnp.bfloat16).reshape(n, capacity, -1)

    raw, qdec, state, decay, returned = moe(
        n,
        packed,
        state_probe_logits,
        retention_logits,
        state_source_entries,
        retention_bound_margin[None, :],
        extra_fading_amount,
        specialist_switch_matrix[0],
        specialist_widen_matrix[0],
        specialist_contract_matrix[0],
    )
    mixer_out = mixer(
        n,
        raw,
        qdec,
        state_result_switch_logits,
        state,
        decay,
        state_result_scale[None, :],
        state_result_matrix,
    )

    flat = returned.reshape(-1, returned.shape[2])
    spread = jnp.sum(jnp.where(hits, own_weight[:, :, None], 0.0), axis=1)
    high = spread.astype(jnp.bfloat16)
    low = (spread - high.astype(jnp.float32)).astype(jnp.bfloat16)
    combined = jnp.dot(high, flat, preferred_element_type=jnp.float32) + jnp.dot(
        low, flat, preferred_element_type=jnp.float32
    )
    moe_out = rms_scale(combined, trailing_scale_vector).astype(jnp.bfloat16)
    return (mixer_out, moe_out)


def solution(mesh):
    return jax.shard_map(
        shards,
        mesh=mesh,
        in_specs=(
            P("ep", "tp"),
            P("ep", "tp"),
            P("ep", "tp"),
            P("ep", "tp"),
            P("tp"),
            P("ep", "tp"),
            P("tp"),
            P(None, "tp"),
            P("ep", None),
            P("ep", None),
            P("ep", None),
            P(),
            P(),
            P("ep", None, "tp"),
            P("ep", None, "tp"),
            P("ep", "tp", None),
        ),
        out_specs=(P("ep", "tp"), P(("ep", "tp"), None)),
        check_vma=False,
    )
```

profile of v0, /device:TPU:0, one launch (start us, length us, event | category | flops | bytes accessed | tf_op | source)
XLA Modules:
  0.0 178.1 jit_solution(9073756842983463268)
XLA Ops:
  0.6 0.0 copy-start
  0.6 0.0 copy-start.9
  0.7 0.7 constant_dynamic-slice_fusion.1
  1.4 0.2 fusion.11
  1.6 0.7 convert_add_fusion
  2.3 0.1 fusion.6
  2.4 1.2 fusion
  3.7 3.2 %convolution_convert_fusion = bf16[512,2048]{1,0:T(8,128)(2,1)} fusion(pred[128,512]{1,0:T(8,128)(4,1)S(1)} %fusion.6, f32[2048]{0:T(1024)} %param.27, f32[128]{0:T(128)S(1)} %add_rsqrt_fusion.1, bf16[512,2048]{1,0:T(8,128)(2,1)} %param.24, s32[]{:T(128)S(6)} %select_n.13), kind=kOutput, calls=%fused_computation | convolution fusion | flops 270532608 | bytes 2695684 | tf_op jit(solution)/shard_map/dot_general | solution.py:489
  6.9 0.0 copy-done.9
  6.9 1.0 copy.23.extra
  7.9 137.7 %moe.1 = (f32[1024,256]{1,0:T(8,128)}, bf16[1024,256]{1,0:T(8,128)(2,1)}, bf16[2,128,128]{2,1,0:T(8,128)(2,1)}, f32[8,256]{1,0:T(8,128)}, bf16[8,64,2048]{2,1,0:T(8,128)(2,1)}) custom-call(bf16[8,64,2048]{2,1,0:T(8,128)(2,1)} %bitcast.14, bf16[1024,256]{1,0:T(8,128)(2,1)} %probe.1, bf16[1024,256]{1,0:T(8,128)(2,1)} %ret.1, bf16[1024,256]{1,0:T(8,128)(2,1)} %val.1, ...), custom_call_target="tpu_custom_call" | custom-call | flops 10000000000 | bytes 200000000 | tf_op jit(solution)/shard_map/moe/pallas_call | solution.py:273
  145.6 0.0 copy-start.8
  145.6 0.0 copy-done
  145.6 0.1 select_reduce_fusion
  145.8 2.2 %fusion.9 = f32[128,2048]{1,0:T(8,128)S(1)} fusion(bf16[512,2048]{1,0:T(8,128)(2,1)} %bitcast.12, f32[128,512]{1,0:T(8,128)S(1)} %select_reduce_fusion), kind=kOutput, calls=%fused_computation.17 | convolution fusion | flops 268500992 | bytes 3407872 | tf_op jit(solution)/shard_map/dot_general | solution.py:519
  147.9 0.0 copy-done.8
  148.0 0.0 copy-start.10
  148.0 0.0 copy-start.1
  148.0 0.0 copy-start.2
  148.0 0.0 copy-start.3
  148.0 0.0 copy-start.4
  148.0 0.0 copy-start.5
  148.0 0.0 copy-start.6
  148.0 0.0 copy-start.7
  148.0 0.6 multiply_reduce_fusion
  148.6 0.0 copy-done.10
  148.7 0.9 multiply_convert_fusion
  149.6 0.0 copy-done.1
  149.6 0.0 copy-done.2
  149.6 0.0 copy-done.3
  149.7 0.3 copy-done.4
  150.0 0.0 copy-done.5
  150.0 0.0 copy-done.6
  150.0 0.0 copy-done.7
  150.0 27.1 %mixer.1 = bf16[1024,512]{1,0:T(8,128)(2,1)S(1)} custom-call(f32[1024,256]{1,0:T(8,128)S(1)} %copy-done.2, bf16[1024,256]{1,0:T(8,128)(2,1)S(1)} %copy-done.4, bf16[1024,256]{1,0:T(8,128)(2,1)S(1)} %copy-done.3, bf16[2,128,128]{2,1,0:T(8,128)(2,1)S(1)} %copy-done.5, f32[8,256]{1,0:T(8,128)S(1)} %copy-done.6, f32[1,256]{1,0:T(1,128)S(1)} %bitcast.11, ...), custom_call_target="tpu_custom_call" | custom-call | flops 1000000000 | bytes 60000000 | tf_op jit(solution)/shard_map/mixer/pallas_call | solution.py:415
  177.1 1.0 copy.25
  (6 shorter events, 0.1 us)
Async XLA Ops:
  0.6 145.0 %copy-start = (f32[512,2]{0,1:T(2,128)S(1)}, f32[512,2]{0,1:T(2,128)}, u32[]{:S(2)}) copy-start(f32[512,2]{0,1:T(2,128)} %param.26) | copy-start | bytes 12292
  0.6 6.2 %copy-start.9 = (f32[1024,2]{0,1:T(2,128)S(1)}, f32[1024,2]{0,1:T(2,128)}, u32[]{:S(2)}) copy-start(f32[1024,2]{0,1:T(2,128)} %param.21) | copy-start | bytes 24580
  145.6 2.4 %copy-start.8 = (bf16[8,64,2048]{2,1,0:T(8,128)(2,1)S(1)}, bf16[8,64,2048]{2,1,0:T(8,128)(2,1)}, u32[]{:S(2)}) copy-start(bf16[8,64,2048]{2,1,0:T(8,128)(2,1)} %get-tuple-element.11) | copy-start | bytes 6291460
  148.0 0.7 copy-start.10
  148.0 1.6 copy-start.1
  148.0 1.6 copy-start.2
  148.0 1.7 copy-start.3
  148.0 2.0 %copy-start.4 = (bf16[1024,256]{1,0:T(8,128)(2,1)S(1)}, bf16[1024,256]{1,0:T(8,128)(2,1)}, u32[]{:S(2)}) copy-start(bf16[1024,256]{1,0:T(8,128)(2,1)} %get-tuple-element.8.qdec) | copy-start | bytes 1572868
  148.0 2.0 %copy-start.5 = (bf16[2,128,128]{2,1,0:T(8,128)(2,1)S(1)}, bf16[2,128,128]{2,1,0:T(8,128)(2,1)}, u32[]{:S(2)}) copy-start(bf16[2,128,128]{2,1,0:T(8,128)(2,1)} %get-tuple-element.9.state) | copy-start | bytes 196612
  148.0 2.0 %copy-start.6 = (f32[8,256]{1,0:T(8,128)S(1)}, f32[8,256]{1,0:T(8,128)}, u32[]{:S(2)}) copy-start(f32[8,256]{1,0:T(8,128)} %get-tuple-element.10.decay) | copy-start | bytes 24580
  148.0 2.0 %copy-start.7 = (f32[256]{0:T(256)S(1)}, f32[256]{0:T(256)}, u32[]{:S(2)}) copy-start(f32[256]{0:T(256)} %param.22) | copy-start | bytes 3076
where the time goes:
time: 180 us; the launch traced here: 178 us
  Pallas kernels  165 us (92%)
  matrix products  6.14 us (3%)
  local copies, waits for them, and re-layouts  3.18 us (2%)
  other arithmetic  3.18 us (2%)
    pallas_call x1, Pallas kernels, moe(): pl.pallas_call(functools.partial(moe_kernel, n), name='moe', out_shape=(j...  138 us
    pallas_call x1, Pallas kernels, mixer(): pl.pallas_call(functools.partial(mixer_kernel, n, chunks), name='mixer',...  27.1 us

commit v1 on v0

v1 whole, which is shorter than its diff:
```python
import functools

import jax
import jax.numpy as jnp
from jax import lax
from jax.experimental import pallas as pl
from jax.experimental.pallas import tpu as pltpu
from jax.sharding import PartitionSpec as P

HEAD = 128
SPAN = 128
TOK_DEV = 128
STAGES = 4
PIECES = 4
STEP = 512
TILE = 16

NORM_EPS = 1e-06
SWISH_ALPHA = 1.702
CLAMP_LIMIT = 7.0
MESH = pl.DeviceIdType.MESH
VMEM = pltpu.VMEM
DMA = pltpu.SemaphoreType.DMA
NT = (((1,), (1,)), ((), ()))
TN = (((0,), (0,)), ((), ()))


def remote(src, dst, send, recv, where):
    return pltpu.make_async_remote_copy(
        src_ref=src, dst_ref=dst, send_sem=send, recv_sem=recv, device_id=where, device_id_type=MESH
    )


def clamped_unit(gate, upward):
    glued = jnp.minimum(gate, CLAMP_LIMIT)
    linear = jnp.clip(upward, -CLAMP_LIMIT, CLAMP_LIMIT)
    return glued * jax.nn.sigmoid(SWISH_ALPHA * glued) * (linear + 1.0)


def rms_scale(values, gain):
    return values * lax.rsqrt(jnp.mean(values * values, axis=-1, keepdims=True) + NORM_EPS) * gain


def span_step(t, probe, ret, val, margin, extra, raw, qdec, state, running):
    rows = pl.ds(pl.multiple_of(t * SPAN, SPAN), SPAN)
    width = probe.shape[1]
    x = probe[rows, :].astype(jnp.float32)
    q = x * jax.nn.sigmoid(x) * HEAD ** (-0.5)
    k = margin[...] * jax.nn.sigmoid(-ret[rows, :].astype(jnp.float32))
    logs = jnp.log1p(-k)
    row = lax.broadcasted_iota(jnp.int32, (SPAN, SPAN), 0)
    col = lax.broadcasted_iota(jnp.int32, (SPAN, SPAN), 1)
    causal = row >= col
    tril = jnp.where(causal, 1.0, 0.0).astype(jnp.float32)
    for h in range(width // HEAD):
        cols = slice(h * HEAD, (h + 1) * HEAD)
        qh, kh = q[:, cols], k[:, cols]
        fade = jnp.transpose(jnp.broadcast_to(extra[h : h + 1, rows], (SPAN, SPAN)))
        ld = logs[:, cols] + fade
        cum = jnp.dot(
            tril, ld, precision=lax.Precision.HIGHEST, preferred_element_type=jnp.float32
        )
        middle = cum[SPAN // 2 - 1 : SPAN // 2, :]
        last = cum[SPAN - 1 :, :]
        a = (qh * jnp.exp(cum - middle)).astype(jnp.bfloat16)
        b = (kh * jnp.exp(middle - cum)).astype(jnp.bfloat16)
        qe = qh * jnp.exp(cum)
        kd = (kh * jnp.exp(last - cum)).astype(jnp.bfloat16)
        v = val[rows, cols]
        s = lax.dot_general(a, b, NT, preferred_element_type=jnp.float32)
        s = jnp.where(causal, s, 0.0).astype(jnp.bfloat16)
        st = state[h]
        out = jnp.dot(s, v, preferred_element_type=jnp.float32)
        out = out + lax.dot_general(
            qe.astype(jnp.bfloat16), st.astype(jnp.bfloat16), NT, preferred_element_type=jnp.float32
        )
        raw[rows, cols] = out
        before = running[0:1, cols]
        qdec[rows, cols] = (qe * jnp.exp(before)).astype(jnp.bfloat16)
        state[h] = jnp.exp(last) * st + lax.dot_general(
            v, kd, TN, preferred_element_type=jnp.float32
        )
        running[:, cols] = running[:, cols] + last


def kernel(
    n, planes, capacity, experts, table, margin, extra, scale, lead, trail,
    tok_hbm, probe_hbm, ret_hbm, val_hbm, switch_hbm, mix_hbm, gate_hbm, up_hbm, down_hbm,
    mix_out, moe_out,
    nt, probe, ret, val, switch, mix_w, gate_w, up_w, down_w,
    rk, sh, meta, relay, rows, part, acc, sendb, recvb, fin, back, pk, pko, comb, spread,
    raw, qdec, state, state_bf, running, plst, pld, chain_in, chain_out, enter, carry, gath,
    load_sem,
    fsend, frecv, msend, mrecv, ysend, yrecv, zsend, zrecv,
    xsend, xrecv, csend, crecv, dsend, drecv,
    esend0, erecv0, esend1, erecv1, bsend, brecv, rsend, rrecv,
    pssend, psrecv, pdsend, pdrecv, chsend, chrecv,
    gxsend, gxrecv, gcsend, gcrecv, gdsend, gdrecv,
):
    i, j = lax.axis_index("ep"), lax.axis_index("tp")
    mate = j + 1 - 2 * (j % 2)
    cross = (j + 2) % 4
    mate_cross = (mate + 2) % 4
    group = n // planes
    p, g = i // group, i % group
    features = nt.shape[2]
    heads = state.shape[0]
    width = probe.shape[1]
    length = probe.shape[0]
    f32, bf = jnp.float32, jnp.bfloat16

    pairs = (
        (tok_hbm, nt), (probe_hbm, probe), (ret_hbm, ret), (val_hbm, val),
        (gate_hbm, gate_w), (up_hbm, up_w), (down_hbm, down_w),
        (switch_hbm, switch), (mix_hbm, mix_w),
    )
    loads = [pltpu.make_async_copy(a, b, load_sem.at[w]) for w, (a, b) in enumerate(pairs)]
    for load in loads:
        load.start()

    barrier = pltpu.get_barrier_semaphore()

    def hello(s, c):
        pl.semaphore_signal(barrier, inc=1, device_id=((i + s) % n, j), device_id_type=MESH)
        return c

    lax.fori_loop(1, n, hello, 0)
    for t in (mate, cross):
        pl.semaphore_signal(barrier, inc=1, device_id=(i, t), device_id_type=MESH)

    def plane(s):
        left, right = p, planes - 1 - p
        big = (left - right + planes) // planes
        small = big * right + (1 - big) * left
        t = s - 1 + 2 * planes
        both = 1 - (t - 2 * small) // (2 * planes)
        t = t - 2 * planes
        far = both * ((t + 2) // 2) + (1 - both) * (s - small)
        sign = (2 * big - 1) * (2 * both * (s % 2) - 1)
        other = (s + planes - 1) // planes - s // planes
        return p + other * sign * far

    def place(c):
        s = (c + 1) // group
        q = plane(s)
        return s, q, q * group + (g + (c + 1) % group) % group

    def ranks():
        ids = lax.broadcasted_iota(jnp.int32, (experts, TOK_DEV), 0).astype(f32)
        one = lax.broadcasted_iota(jnp.int32, (TOK_DEV, TOK_DEV), 0)
        two = lax.broadcasted_iota(jnp.int32, (TOK_DEV, TOK_DEV), 1)
        earlier = jnp.where(one < two, 1.0, 0.0).astype(bf)
        top = table.shape[0] // 2
        for b in range(4):
            lanes = slice(b * TOK_DEV, (b + 1) * TOK_DEV)
            named = jnp.zeros((experts, TOK_DEV), f32)
            share = jnp.zeros((experts, TOK_DEV), f32)
            for w in range(top):
                hit = ids == table[w : w + 1, lanes]
                named = named + jnp.where(hit, 1.0, 0.0)
                share = share + jnp.where(hit, table[top + w : top + w + 1, lanes], 0.0)
            ahead = jnp.dot(named.astype(bf), earlier, preferred_element_type=f32)
            rk[b] = jnp.where(named > 0.5, ahead, -1.0)
            sh[b] = share

    def norm(b):
        def tile(t, c):
            r = pl.ds(pl.multiple_of(t * TILE, TILE), TILE)
            nt[b, r, :] = rms_scale(nt[b, r, :].astype(f32), lead[...]).astype(bf)
            return c

        lax.fori_loop(0, TOK_DEV // TILE, tile, 0)

    slot = lax.broadcasted_iota(jnp.int32, (capacity, TOK_DEV), 0).astype(f32)

    def one_hot(ranked, e):
        return jnp.where(slot == ranked[pl.ds(e, 1), :], 1.0, 0.0)

    def pack(ranked, tokens, own, others):
        picks = [one_hot(ranked, i)]
        if others is not None:
            picks += [one_hot(ranked, p * group + (g + r) % group) for r in range(1, group)]
        pick = (picks[0] if len(picks) == 1 else jnp.concatenate(picks, axis=0)).astype(bf)
        for f in range(0, features, STEP):
            y = jnp.dot(pick, tokens[:, f : f + STEP], preferred_element_type=f32).astype(bf)
            own[:, f : f + STEP] = y[:capacity]
            for r in range(1, len(picks)):
                others[r - 1, :, f : f + STEP] = y[r * capacity : (r + 1) * capacity]

    def step_right(q, src, info):
        return (
            remote(src, relay.at[q], fsend.at[0, q], frecv.at[q], (i + group, j)),
            remote(info, meta.at[q], msend.at[0, q], mrecv.at[q], (i + group, j)),
        )

    def step_left(q, src, info):
        return (
            remote(src, relay.at[q], fsend.at[1, q], frecv.at[q], (i - group, j)),
            remote(info, meta.at[q], msend.at[1, q], mrecv.at[q], (i - group, j)),
        )

    def over_y(q, r):
        k = q * group + g
        d = p * group + (g + r) % group
        return remote(pk.at[q, r - 1], rows.at[k, j], ysend.at[q, r], yrecv.at[k], (d, j))

    def got_y(k):
        return remote(pk.at[0, 0], rows.at[k, j], ysend.at[0, 0], yrecv.at[k], (i, mate))

    def near(r, w):
        d = p * group + (g + r) % group
        b = (j, cross)[w]
        return remote(pko.at[w, r - 1], rows.at[i, b], zsend.at[w, r], zrecv.at[w, i], (d, j))

    def got_near(k, w):
        b = (j, cross)[w]
        return remote(pko.at[w, 0], rows.at[k, b], zsend.at[w, 0], zrecv.at[w, k], (i, mate))

    def over_x(k):
        return remote(rows.at[k, j], rows.at[k, j], xsend.at[k], xrecv.at[k], (i, cross))

    def over_c(k):
        return remote(rows.at[k, j], rows.at[k, j], csend.at[k], crecv.at[k], (i, mate))

    def over_d(k):
        return remote(rows.at[k, cross], rows.at[k, cross], dsend.at[k], drecv.at[k], (i, mate))

    def to_mate(k, close):
        if close:
            return remote(part.at[k, mate], acc.at[0, k], esend0.at[k], erecv0.at[k], (i, mate))
        return remote(
            part.at[k, mate_cross], acc.at[1, k], esend1.at[k], erecv1.at[k], (i, mate)
        )

    def to_cross(k):
        return remote(sendb.at[k], recvb.at[k], bsend.at[k], brecv.at[k], (i, cross))

    def home(k):
        return remote(fin.at[k], back.at[i], rsend.at[k], rrecv.at[i], (k, j))

    def home_in(k):
        return remote(fin.at[k], back.at[k], rsend.at[k], rrecv.at[k], (k, j))

    def arrive(s):
        q = plane(s)
        k = q * group + g
        for copy in step_right(q, relay.at[q], meta.at[q]):
            copy.wait_recv()

        @pl.when((q < p) & (p + 1 < planes))
        def _():
            for copy in step_right(q, relay.at[q], meta.at[q]):
                copy.start()

        @pl.when((q > p) & (p >= 1))
        def _():
            for copy in step_left(q, relay.at[q], meta.at[q]):
                copy.start()

        pack(meta.at[q], relay.at[q], rows.at[k, j], pk.at[q])
        over_x(k).start()
        over_c(k).start()
        for r in range(1, group):
            over_y(q, r).start()

    def arrive_y(s):
        q = plane(s)
        for r in range(1, group):
            k = q * group + (g + r) % group
            got_y(k).wait_recv()
            over_x(k).start()
            over_c(k).start()

    def work(c):
        s, q, k = place(c)

        @pl.when((s >= 1) & (s < planes))
        def _():
            over_x(k).wait_recv()
            over_d(k).start()

        @pl.when(s < planes)
        def _():
            over_c(k).wait_recv()
            over_d(k).wait_recv()

        x = rows[k].reshape(4 * capacity, features)
        gate = jnp.dot(x, gate_w[...], preferred_element_type=f32)
        upward = jnp.dot(x, up_w[...], preferred_element_type=f32)
        act = clamped_unit(gate, upward).astype(bf)
        for f in range(0, features, STEP):
            y = jnp.dot(act, down_w[:, f : f + STEP], preferred_element_type=f32)
            part[k, :, :, f : f + STEP] = y.astype(bf).reshape(4, capacity, STEP)
        to_mate(k, False).start()
        to_mate(k, True).start()

    def first_sum(c):
        s, q, k = place(c)
        to_mate(k, False).wait()
        x = part[k, cross].astype(f32) + acc[1, k].astype(f32)
        sendb[k] = x.astype(bf)
        to_cross(k).start()

    def total(c):
        s, q, k = place(c)
        to_mate(k, True).wait()
        to_cross(k).wait()
        x = part[k, j].astype(f32) + acc[0, k].astype(f32)
        fin[k] = (x + recvb[k].astype(f32)).astype(bf)

        @pl.when(s < planes)
        def _():
            home(k).start()

    def in_plane(r):
        d = p * group + (g + r) % group
        return (
            remote(state_bf, plst.at[g], pssend.at[r], psrecv.at[g], (d, j)),
            remote(running, pld.at[g], pdsend.at[r], pdrecv.at[g], (d, j)),
        )

    def in_plane_got(r):
        o = (g + r) % group
        return (
            remote(state_bf, plst.at[o], pssend.at[r], psrecv.at[o], (i, mate)),
            remote(running, pld.at[o], pdsend.at[r], pdrecv.at[o], (i, mate)),
        )

    def chain():
        return remote(chain_out, chain_in, chsend, chrecv, (i + group, j))

    def prefix():
        for r in range(1, group):
            for copy in in_plane_got(r):
                copy.wait_recv()

        @pl.when(p == 0)
        def _():
            carry[...] = jnp.zeros_like(carry)

        @pl.when(p >= 1)
        def _():
            chain().wait_recv()
            carry[...] = chain_in[...].astype(f32)

        for o in range(group):
            @pl.when(g == o)
            def _():
                enter[...] = carry[...]

            for h in range(heads):
                d = pld[o, 0:1, h * HEAD : (h + 1) * HEAD]
                carry[h] = jnp.exp(d) * carry[h] + plst[o, h].astype(f32)

        @pl.when(p + 1 < planes)
        def _():
            chain_out[...] = carry[...].astype(bf)
            chain().start()

    piece = length // PIECES

    def at(c):
        return pl.ds(pl.multiple_of(c * piece, piece), piece)

    def mix_x(c):
        here = gath.at[j, at(c)]
        return remote(here, here, gxsend.at[c], gxrecv.at[c], (i, cross))

    def mix_c(c):
        here = gath.at[j, at(c)]
        return remote(here, here, gcsend.at[c], gcrecv.at[c], (i, mate))

    def mix_d(c):
        here = gath.at[cross, at(c)]
        return remote(here, here, gdsend.at[c], gdrecv.at[c], (i, mate))

    def mix_final(c, z):
        r = at(c)
        for h in range(heads):
            cols = slice(h * HEAD, (h + 1) * HEAD)
            x = raw[r, cols] + lax.dot_general(
                qdec[r, cols], enter[h].astype(bf), NT, preferred_element_type=f32
            )
            x = x * lax.rsqrt(jnp.mean(x * x, axis=-1, keepdims=True) + NORM_EPS)
            v = switch[r, cols].astype(f32)
            gath[j, r, cols] = (x * scale[:, cols] * (v * jax.nn.sigmoid(v))).astype(bf)
        mix_x(c).start()
        mix_c(c).start()
        return z

    def mix_pass(c, z):
        mix_x(c).wait()
        mix_d(c).start()
        return z

    def mix_project(c, z):
        mix_c(c).wait()
        mix_d(c).wait()
        r = at(c)
        a = jnp.dot(gath[0, r, :], mix_w[0:width, :], preferred_element_type=f32)
        for w in range(1, 4):
            a = a + jnp.dot(
                gath[w, r, :], mix_w[w * width : (w + 1) * width, :], preferred_element_type=f32
            )
        mix_out[r, :] = a.astype(bf)
        return z

    ranks()
    loads[0].wait()
    norm(j)
    pl.semaphore_wait(barrier, n + 1)

    @pl.when(p + 1 < planes)
    def _():
        for copy in step_right(p, nt.at[j], rk.at[j]):
            copy.start()

    @pl.when(p >= 1)
    def _():
        for copy in step_left(p, nt.at[j], rk.at[j]):
            copy.start()

    norm(cross)
    for w, b in enumerate((j, cross)):
        pack(rk.at[b], nt.at[b], rows.at[i, b], pko.at[w])
        for r in range(1, group):
            near(r, w).start()
    norm(mate)
    norm(mate_cross)
    for b in (mate, mate_cross):
        pack(rk.at[b], nt.at[b], rows.at[i, b], None)

    for load in loads[1:4]:
        load.wait()
    state[...] = jnp.zeros_like(state)
    running[...] = jnp.zeros_like(running)

    def spans(t, c):
        span_step(t, probe, ret, val, margin, extra, raw, qdec, state, running)
        return c

    lax.fori_loop(0, length // SPAN, spans, 0)
    for h in range(heads):
        state_bf[h] = state[h].astype(bf)
    plst[g] = state_bf[...]
    pld[g] = running[...]
    for r in range(1, group):
        for copy in in_plane(r):
            copy.start()
    for r in range(1, group):
        k = p * group + (g + r) % group
        got_near(k, 0).wait_recv()
        over_c(k).start()
        got_near(k, 1).wait_recv()
        over_d(k).start()
    for load in loads[4:]:
        load.wait()

    def pump(u, z):
        @pl.when(u < planes - 1)
        def _():
            arrive(u + 1)

        @pl.when(u < n)
        def _():
            work(u)

        @pl.when((u >= 1) & (u < n + 1))
        def _():
            first_sum(u - 1)

        @pl.when((u >= 2) & (u < n + 2))
        def _():
            total(u - 2)

        @pl.when(u == 0)
        def _():
            prefix()

        @pl.when(u < planes - 1)
        def _():
            arrive_y(u + 1)

        @pl.when(u == planes - 1)
        def _():
            lax.fori_loop(0, PIECES, mix_final, 0)

        @pl.when(u == planes)
        def _():
            lax.fori_loop(0, PIECES, mix_pass, 0)

        @pl.when(u == planes + 1)
        def _():
            lax.fori_loop(0, PIECES, mix_project, 0)

        return z

    lax.fori_loop(0, n + 2, pump, 0)
    back[i] = fin[i]

    def weigh(e, z):
        r = pl.ds(pl.multiple_of(e * capacity, capacity), capacity)
        spread[r, :] = jnp.where(
            slot == rk[j, pl.ds(e, 1), :], jnp.broadcast_to(sh[j, pl.ds(e, 1), :], slot.shape), 0.0
        )
        return z

    lax.fori_loop(0, experts, weigh, 0)
    wide = spread[...]
    high = wide.astype(bf)
    low = (wide - high.astype(f32)).astype(bf)

    def collect(s, z):
        k = (i + s) % n
        home_in(k).wait_recv()
        return z

    lax.fori_loop(1, n, collect, 0)
    for f in range(0, features, STEP):
        flat = back[:, :, f : f + STEP].reshape(n * capacity, STEP)
        comb[:, f : f + STEP] = lax.dot_general(
            high, flat, TN, preferred_element_type=f32
        ) + lax.dot_general(low, flat, TN, preferred_element_type=f32)

    def closing(t, z):
        r = pl.ds(pl.multiple_of(t * TILE, TILE), TILE)
        moe_out[r, :] = rms_scale(comb[r, :], trail[...]).astype(bf)
        return z

    lax.fori_loop(0, TOK_DEV // TILE, closing, 0)

    def finish(s, z):
        k = (i + s) % n
        over_c(k).wait_send()
        over_d(k).wait_send()
        home(k).wait_send()
        return z

    lax.fori_loop(1, n, finish, 0)

    def finish_far(s, z):
        q = plane(s)
        for r in range(group):
            over_x(q * group + r).wait_send()
        for r in range(1, group):
            over_y(q, r).wait_send()

        @pl.when((q < p) & (p + 1 < planes))
        def _():
            for copy in step_right(q, relay.at[q], meta.at[q]):
                copy.wait_send()

        @pl.when((q > p) & (p >= 1))
        def _():
            for copy in step_left(q, relay.at[q], meta.at[q]):
                copy.wait_send()

        return z

    lax.fori_loop(1, planes, finish_far, 0)

    @pl.when(p + 1 < planes)
    def _():
        for copy in step_right(p, nt.at[j], rk.at[j]):
            copy.wait_send()
        chain().wait_send()

    @pl.when(p >= 1)
    def _():
        for copy in step_left(p, nt.at[j], rk.at[j]):
            copy.wait_send()

    for r in range(1, group):
        for w in range(2):
            near(r, w).wait_send()
        for copy in in_plane(r):
            copy.wait_send()


def shards(
    state_probe_logits,
    retention_logits,
    state_source_entries,
    state_result_switch_logits,
    retention_bound_margin,
    extra_fading_amount,
    state_result_scale,
    state_result_matrix,
    second_slice_tokens,
    specialist_assignment,
    selected_specialist_share,
    leading_scale_vector,
    trailing_scale_vector,
    specialist_switch_matrix,
    specialist_widen_matrix,
    specialist_contract_matrix,
):
    n = lax.axis_size("ep")
    experts = specialist_switch_matrix.shape[0] * n
    top_count = specialist_assignment.shape[1]
    capacity = 2 * TOK_DEV * top_count // experts
    planes = max(d for d in range(1, STAGES + 1) if n % d == 0)
    group = n // planes
    length, width = state_probe_logits.shape
    heads = width // HEAD
    features = second_slice_tokens.shape[1]
    hidden = specialist_switch_matrix.shape[2]
    columns = state_result_matrix.shape[1]
    bf, f32 = jnp.bfloat16, jnp.float32
    table = jnp.concatenate(
        [specialist_assignment.astype(f32), selected_specialist_share], axis=1
    ).T
    vm = pl.BlockSpec(memory_space=VMEM)
    hbm = pl.BlockSpec(memory_space=pl.ANY)
    chunk = (capacity, features)
    block = (TOK_DEV, features)
    return tuple(
        pl.pallas_call(
            functools.partial(kernel, n, planes, capacity, experts),
            name="fused",
            out_shape=(
                jax.ShapeDtypeStruct((length, columns), bf),
                jax.ShapeDtypeStruct(block, bf),
            ),
            in_specs=[vm] * 6 + [hbm] * 9,
            out_specs=(vm, vm),
            scratch_shapes=[
                VMEM((4,) + block, bf),
                VMEM((length, width), bf),
                VMEM((length, width), bf),
                VMEM((length, width), bf),
                VMEM((length, width), bf),
                VMEM(state_result_matrix.shape, bf),
                VMEM((features, hidden), bf),
                VMEM((features, hidden), bf),
                VMEM((hidden, features), bf),
                VMEM((4, experts, TOK_DEV), f32),
                VMEM((4, experts, TOK_DEV), f32),
                VMEM((planes, experts, TOK_DEV), f32),
                VMEM((planes,) + block, bf),
                VMEM((n, 4) + chunk, bf),
                VMEM((n, 4) + chunk, bf),
                VMEM((2, n) + chunk, bf),
                VMEM((n,) + chunk, bf),
                VMEM((n,) + chunk, bf),
                VMEM((n,) + chunk, bf),
                VMEM((n,) + chunk, bf),
                VMEM((planes, group - 1) + chunk, bf),
                VMEM((2, group - 1) + chunk, bf),
                VMEM(block, f32),
                VMEM((n * capacity, TOK_DEV), f32),
                VMEM((length, width), f32),
                VMEM((length, width), bf),
                VMEM((heads, HEAD, HEAD), f32),
                VMEM((heads, HEAD, HEAD), bf),
                VMEM((8, width), f32),
                VMEM((group, heads, HEAD, HEAD), bf),
                VMEM((group, 8, width), f32),
                VMEM((heads, HEAD, HEAD), bf),
                VMEM((heads, HEAD, HEAD), bf),
                VMEM((heads, HEAD, HEAD), f32),
                VMEM((heads, HEAD, HEAD), f32),
                VMEM((4, length, width), bf),
                DMA((9,)),
                DMA((2, planes)), DMA((planes,)), DMA((2, planes)), DMA((planes,)),
                DMA((planes, group)), DMA((n,)), DMA((2, group)), DMA((2, n)),
            ]
            + [DMA((n,))] * 14
            + [DMA((group,))] * 4
            + [DMA, DMA]
            + [DMA((PIECES,))] * 6,
            compiler_params=pltpu.CompilerParams(
                collective_id=0, has_side_effects=True, vmem_limit_bytes=62 * 2**20
            ),
        )(
            table,
            retention_bound_margin[None, :],
            extra_fading_amount.T,
            state_result_scale[None, :],
            leading_scale_vector[None, :],
            trailing_scale_vector[None, :],
            second_slice_tokens.reshape((4,) + block),
            state_probe_logits,
            retention_logits,
            state_source_entries,
            state_result_switch_logits,
            state_result_matrix,
            specialist_switch_matrix[0],
            specialist_widen_matrix[0],
            specialist_contract_matrix[0],
        )
    )


def solution(mesh):
    return jax.shard_map(
        shards,
        mesh=mesh,
        in_specs=(
            P("ep", "tp"),
            P("ep", "tp"),
            P("ep", "tp"),
            P("ep", "tp"),
            P("tp"),
            P("ep", "tp"),
            P("tp"),
            P(None, "tp"),
            P("ep", None),
            P("ep", None),
            P("ep", None),
            P(),
            P(),
            P("ep", None, "tp"),
            P("ep", None, "tp"),
            P("ep", "tp", None),
        ),
        out_specs=(P("ep", "tp"), P(("ep", "tp"), None)),
        check_vma=False,
    )
```

time: 180 us -> 155 us (0.86)
  Pallas kernels: 165 us -> 149 us
  matrix products: 6.14 us -> 0 us
    pallas_call x2 -> x1, Pallas kernels: 165 us -> 149 us  [shards(): pl.pallas_call(functools.partial(kernel, n, planes, capacity, experts), n...]
    dot_general x4 -> x0, matrix products: 6.14 us -> none  [the longest x1 3.23 us: shards(): lax.dot_general(pick, normed, TN, preferred_element_type=jnp.float32)]
where the time goes in v1:
time: 155 us
  Pallas kernels  149 us (96%)
  local copies, waits for them, and re-layouts  3.12 us (2%)
  other arithmetic  1.98 us (1%)
    pallas_call x1, Pallas kernels, shards(): pl.pallas_call(functools.partial(kernel, n, planes, capacity, experts), n...  149 us
    unnamed x4, local copies, waits for them, and re-layouts  3.12 us

profile of v1, /device:TPU:0, one launch (start us, length us, event | category | flops | bytes accessed | tf_op | source)
XLA Modules:
  0.0 154.9 jit_solution(16339814739303801460)
XLA Ops:
  0.6 0.7 convert_element_type.3
  1.3 1.3 maximum_bitcast_fusion.table
  2.6 149.2 %fused.1 = (bf16[1024,512]{1,0:T(8,128)(2,1)}, bf16[128,2048]{1,0:T(8,128)(2,1)}) custom-call(f32[4,512]{1,0:T(4,128)} %maximum_bitcast_fusion.table, f32[1,256]{1,0:T(1,128)} %bitcast.18, f32[2,1024]{1,0:T(2,128)} %bitcast.15, f32[1,256]{1,0:T(1,128)} %bitcast.19, f32[1,2048]{1,0:T(1,128)} %bitcast.16, f32[1,2048]{1,0:T(1,128)} %bitcast.17, ...), custom_call_target="tpu_custom_call" | custom-call | tf_op jit(solution)/shard_map/fused/pallas_call | solution.py:618
  151.8 0.0 copy-start
  151.8 2.3 %copy.20 = bf16[1024,512]{1,0:T(8,128)(2,1)} copy(bf16[1024,512]{1,0:T(8,128)(2,1)} %get-tuple-element.4) | data formatting | bytes 2097152
  154.1 0.0 copy-done
  154.1 0.8 copy.21
Async XLA Ops:
  151.8 2.3 %copy-start = (bf16[128,2048]{1,0:T(8,128)(2,1)S(1)}, bf16[128,2048]{1,0:T(8,128)(2,1)}, u32[]{:S(2)}) copy-start(bf16[128,2048]{1,0:T(8,128)(2,1)} %get-tuple-element.5) | copy-start | bytes 1572868

commit v2 on v1

--- a/solution.py
+++ b/solution.py
@@ -84,14 +84,14 @@
 
 
 def kernel(
-    n, planes, capacity, experts, table, margin, extra, scale, lead, trail,
+    n, planes, capacity, experts, named_by, shared_by, margin, extra, scale, lead, trail,
     tok_hbm, probe_hbm, ret_hbm, val_hbm, switch_hbm, mix_hbm, gate_hbm, up_hbm, down_hbm,
     mix_out, moe_out,
     nt, probe, ret, val, switch, mix_w, gate_w, up_w, down_w,
-    rk, sh, meta, relay, rows, part, acc, sendb, recvb, fin, back, pk, pko, comb, spread,
+    rk, sh, meta, relay, meta2, relay2, rows, part, acc, sendb, recvb, fin, back, pk, pk2, pko, comb, spread,
     raw, qdec, state, state_bf, running, plst, pld, chain_in, chain_out, enter, carry, gath,
     load_sem,
-    fsend, frecv, msend, mrecv, ysend, yrecv, zsend, zrecv,
+    fsend, frecv, msend, mrecv, ysend, yrecv, zsend, zrecv, tsend, trecv, vsend, vrecv,
     xsend, xrecv, csend, crecv, dsend, drecv,
     esend0, erecv0, esend1, erecv1, bsend, brecv, rsend, rrecv,
     pssend, psrecv, pdsend, pdrecv, chsend, chrecv,
@@ -141,24 +141,26 @@
         return p + other * sign * far
 
     def place(c):
-        s = (c + 1) // group
+        t = (c + 1) // group
+        last = (t + 1) // planes
+        s = t + (t + planes - 1) // planes - last * (planes - 1)
         q = plane(s)
         return s, q, q * group + (g + (c + 1) % group) % group
 
     def ranks():
-        ids = lax.broadcasted_iota(jnp.int32, (experts, TOK_DEV), 0).astype(f32)
+        ids = lax.broadcasted_iota(jnp.int32, (experts, TOK_DEV), 0)
         one = lax.broadcasted_iota(jnp.int32, (TOK_DEV, TOK_DEV), 0)
         two = lax.broadcasted_iota(jnp.int32, (TOK_DEV, TOK_DEV), 1)
         earlier = jnp.where(one < two, 1.0, 0.0).astype(bf)
-        top = table.shape[0] // 2
+        top = named_by.shape[0]
         for b in range(4):
             lanes = slice(b * TOK_DEV, (b + 1) * TOK_DEV)
             named = jnp.zeros((experts, TOK_DEV), f32)
             share = jnp.zeros((experts, TOK_DEV), f32)
             for w in range(top):
-                hit = ids == table[w : w + 1, lanes]
+                hit = ids == named_by[w : w + 1, lanes]
                 named = named + jnp.where(hit, 1.0, 0.0)
-                share = share + jnp.where(hit, table[top + w : top + w + 1, lanes], 0.0)
+                share = share + jnp.where(hit, shared_by[w : w + 1, lanes], 0.0)
             ahead = jnp.dot(named.astype(bf), earlier, preferred_element_type=f32)
             rk[b] = jnp.where(named > 0.5, ahead, -1.0)
             sh[b] = share
@@ -241,24 +243,56 @@
     def home_in(k):
         return remote(fin.at[k], back.at[k], rsend.at[k], rrecv.at[k], (k, j))
 
+    def twin():
+        q = plane(1)
+        return (
+            remote(nt.at[cross], relay2, tsend.at[0], trecv.at[0], (q * group + g, j)),
+            remote(rk.at[cross], meta2, tsend.at[1], trecv.at[1], (q * group + g, j)),
+        )
+
+    def twin_y(r):
+        k = plane(1) * group + g
+        d = p * group + (g + r) % group
+        return remote(pk2.at[r - 1], rows.at[k, cross], vsend.at[r], vrecv.at[k], (d, j))
+
+    def got_twin_y(k):
+        return remote(pk2.at[0], rows.at[k, cross], vsend.at[0], vrecv.at[k], (i, mate))
+
+    inner = (p >= 1) & (p + 1 < planes)
+
+    def forward(s):
+        q = plane(s)
+
+        @pl.when(inner)
+        def _():
+            for copy in step_right(q, relay.at[q], meta.at[q]):
+                copy.wait_recv()
+
+        @pl.when(inner & (q < p))
+        def _():
+            for copy in step_right(q, relay.at[q], meta.at[q]):
+                copy.start()
+
+        @pl.when(inner & (q > p))
+        def _():
+            for copy in step_left(q, relay.at[q], meta.at[q]):
+                copy.start()
+
     def arrive(s):
         q = plane(s)
         k = q * group + g
-        for copy in step_right(q, relay.at[q], meta.at[q]):
-            copy.wait_recv()
-
-        @pl.when((q < p) & (p + 1 < planes))
+
+        @pl.when((p == 0) | (p + 1 == planes))
         def _():
             for copy in step_right(q, relay.at[q], meta.at[q]):
-                copy.start()
-
-        @pl.when((q > p) & (p >= 1))
-        def _():
-            for copy in step_left(q, relay.at[q], meta.at[q]):
-                copy.start()
+                copy.wait_recv()
 
         pack(meta.at[q], relay.at[q], rows.at[k, j], pk.at[q])
-        over_x(k).start()
+
+        @pl.when(s >= 2)
+        def _():
+            over_x(k).start()
+
         over_c(k).start()
         for r in range(1, group):
             over_y(q, r).start()
@@ -268,22 +302,29 @@
         for r in range(1, group):
             k = q * group + (g + r) % group
             got_y(k).wait_recv()
-            over_x(k).start()
+
+            @pl.when(s >= 2)
+            def _():
+                over_x(k).start()
+
             over_c(k).start()
 
-    def work(c):
-        s, q, k = place(c)
-
-        @pl.when((s >= 1) & (s < planes))
-        def _():
-            over_x(k).wait_recv()
+    def arrive_twin():
+        k = plane(1) * group + g
+        for copy in twin():
+            copy.wait_recv()
+        pack(meta2, relay2, rows.at[k, cross], pk2)
+        over_d(k).start()
+        for r in range(1, group):
+            twin_y(r).start()
+
+    def arrive_twin_y():
+        for r in range(1, group):
+            k = plane(1) * group + (g + r) % group
+            got_twin_y(k).wait_recv()
             over_d(k).start()
 
-        @pl.when(s < planes)
-        def _():
-            over_c(k).wait_recv()
-            over_d(k).wait_recv()
-
+    def expert(k):
         x = rows[k].reshape(4 * capacity, features)
         gate = jnp.dot(x, gate_w[...], preferred_element_type=f32)
         upward = jnp.dot(x, up_w[...], preferred_element_type=f32)
@@ -294,23 +335,27 @@
         to_mate(k, False).start()
         to_mate(k, True).start()
 
-    def first_sum(c):
-        s, q, k = place(c)
+    def work(k, s):
+        @pl.when(s >= 2)
+        def _():
+            over_x(k).wait_recv()
+            over_d(k).start()
+
+        over_c(k).wait_recv()
+        over_d(k).wait_recv()
+        expert(k)
+
+    def first_sum(k):
         to_mate(k, False).wait()
         x = part[k, cross].astype(f32) + acc[1, k].astype(f32)
         sendb[k] = x.astype(bf)
         to_cross(k).start()
 
-    def total(c):
-        s, q, k = place(c)
+    def total(k):
         to_mate(k, True).wait()
         to_cross(k).wait()
         x = part[k, j].astype(f32) + acc[0, k].astype(f32)
-        fin[k] = (x + recvb[k].astype(f32)).astype(bf)
-
-        @pl.when(s < planes)
-        def _():
-            home(k).start()
+        return (x + recvb[k].astype(f32)).astype(bf)
 
     def in_plane(r):
         d = p * group + (g + r) % group
@@ -439,7 +484,15 @@
         span_step(t, probe, ret, val, margin, extra, raw, qdec, state, running)
         return c
 
-    lax.fori_loop(0, length // SPAN, spans, 0)
+    half = length // SPAN // 2
+    for load in loads[4:]:
+        load.wait()
+    expert(i)
+    first_sum(i)
+    lax.fori_loop(0, half, spans, 0)
+    if planes > 1:
+        forward(1)
+    lax.fori_loop(half, length // SPAN, spans, 0)
     for h in range(heads):
         state_bf[h] = state[h].astype(bf)
     plst[g] = state_bf[...]
@@ -453,50 +506,62 @@
         over_c(k).start()
         got_near(k, 1).wait_recv()
         over_d(k).start()
-    for load in loads[4:]:
-        load.wait()
+
+    def turn(u):
+        return u - (u + n - group) // n
 
     def pump(u, z):
+        @pl.when(u < planes - 2)
+        def _():
+            forward(u + 2)
+
+        @pl.when(u == 1)
+        def _():
+            for copy in twin():
+                copy.start()
+
+        @pl.when((u < n) & (u != group - 1))
+        def _():
+            s, q, k = place(turn(u))
+            work(k, s)
+            first_sum(k)
+
         @pl.when(u < planes - 1)
         def _():
             arrive(u + 1)
 
-        @pl.when(u < n)
-        def _():
-            work(u)
-
-        @pl.when((u >= 1) & (u < n + 1))
-        def _():
-            first_sum(u - 1)
-
-        @pl.when((u >= 2) & (u < n + 2))
-        def _():
-            total(u - 2)
+        @pl.when((u >= 1) & (u < n + 1) & (u != group))
+        def _():
+            s, q, k = place(turn(u - 1))
+            fin[k] = total(k)
+            home(k).start()
 
         @pl.when(u == 0)
         def _():
+            back[i] = total(i)
             prefix()
 
         @pl.when(u < planes - 1)
         def _():
             arrive_y(u + 1)
 
-        @pl.when(u == planes - 1)
+        @pl.when(u == planes)
+        def _():
+            arrive_twin()
+
+        @pl.when(u == planes + 1)
+        def _():
+            arrive_twin_y()
+
+        @pl.when(u == n - 1)
         def _():
             lax.fori_loop(0, PIECES, mix_final, 0)
 
-        @pl.when(u == planes)
-        def _():
-            lax.fori_loop(0, PIECES, mix_pass, 0)
-
-        @pl.when(u == planes + 1)
-        def _():
-            lax.fori_loop(0, PIECES, mix_project, 0)
-
-        return z
-
-    lax.fori_loop(0, n + 2, pump, 0)
-    back[i] = fin[i]
+        return z
+
+    lax.fori_loop(0, n + 1, pump, 0)
+    lax.fori_loop(0, PIECES, mix_pass, 0)
+    lax.fori_loop(0, PIECES, mix_project, 0)
 
     def weigh(e, z):
         r = pl.ds(pl.multiple_of(e * capacity, capacity), capacity)
@@ -540,8 +605,12 @@
 
     def finish_far(s, z):
         q = plane(s)
-        for r in range(group):
-            over_x(q * group + r).wait_send()
+
+        @pl.when(s >= 2)
+        def _():
+            for r in range(group):
+                over_x(q * group + r).wait_send()
+
         for r in range(1, group):
             over_y(q, r).wait_send()
 
@@ -570,6 +639,11 @@
         for copy in step_left(p, nt.at[j], rk.at[j]):
             copy.wait_send()
 
+    if planes > 1:
+        for copy in twin():
+            copy.wait_send()
+        for r in range(1, group):
+            twin_y(r).wait_send()
     for r in range(1, group):
         for w in range(2):
             near(r, w).wait_send()
@@ -599,7 +673,7 @@
     experts = specialist_switch_matrix.shape[0] * n
     top_count = specialist_assignment.shape[1]
     capacity = 2 * TOK_DEV * top_count // experts
-    planes = max(d for d in range(1, STAGES + 1) if n % d == 0)
+    planes = max(d for d in (1, 2, STAGES) if n % (2 * d) == 0)
     group = n // planes
     length, width = state_probe_logits.shape
     heads = width // HEAD
@@ -607,9 +681,6 @@
     hidden = specialist_switch_matrix.shape[2]
     columns = state_result_matrix.shape[1]
     bf, f32 = jnp.bfloat16, jnp.float32
-    table = jnp.concatenate(
-        [specialist_assignment.astype(f32), selected_specialist_share], axis=1
-    ).T
     vm = pl.BlockSpec(memory_space=VMEM)
     hbm = pl.BlockSpec(memory_space=pl.ANY)
     chunk = (capacity, features)
@@ -622,7 +693,7 @@
                 jax.ShapeDtypeStruct((length, columns), bf),
                 jax.ShapeDtypeStruct(block, bf),
             ),
-            in_specs=[vm] * 6 + [hbm] * 9,
+            in_specs=[vm] * 7 + [hbm] * 9,
             out_specs=(vm, vm),
             scratch_shapes=[
                 VMEM((4,) + block, bf),
@@ -638,6 +709,8 @@
                 VMEM((4, experts, TOK_DEV), f32),
                 VMEM((planes, experts, TOK_DEV), f32),
                 VMEM((planes,) + block, bf),
+                VMEM((experts, TOK_DEV), f32),
+                VMEM(block, bf),
                 VMEM((n, 4) + chunk, bf),
                 VMEM((n, 4) + chunk, bf),
                 VMEM((2, n) + chunk, bf),
@@ -646,6 +719,7 @@
                 VMEM((n,) + chunk, bf),
                 VMEM((n,) + chunk, bf),
                 VMEM((planes, group - 1) + chunk, bf),
+                VMEM((group - 1,) + chunk, bf),
                 VMEM((2, group - 1) + chunk, bf),
                 VMEM(block, f32),
                 VMEM((n * capacity, TOK_DEV), f32),
@@ -664,6 +738,7 @@
                 DMA((9,)),
                 DMA((2, planes)), DMA((planes,)), DMA((2, planes)), DMA((planes,)),
                 DMA((planes, group)), DMA((n,)), DMA((2, group)), DMA((2, n)),
+                DMA((2,)), DMA((2,)), DMA((group,)), DMA((n,)),
             ]
             + [DMA((n,))] * 14
             + [DMA((group,))] * 4
@@ -673,7 +748,8 @@
                 collective_id=0, has_side_effects=True, vmem_limit_bytes=62 * 2**20
             ),
         )(
-            table,
+            specialist_assignment.T,
+            selected_specialist_share.T,
             retention_bound_margin[None, :],
             extra_fading_amount.T,
             state_result_scale[None, :],

time: 155 us -> 131 us (0.85)
  Pallas kernels: 149 us -> 127 us
  other arithmetic: 1.98 us -> 0 us
    pallas_call x1, Pallas kernels: 149 us -> 127 us  [shards(): pl.pallas_call(functools.partial(kernel, n, planes, capacity, experts), n...]
where the time goes in v2:
time: 131 us
  Pallas kernels  127 us (97%)
  local copies, waits for them, and re-layouts  3.12 us (2%)
    pallas_call x1, Pallas kernels, shards(): pl.pallas_call(functools.partial(kernel, n, planes, capacity, experts), n...  127 us
    unnamed x4, local copies, waits for them, and re-layouts  3.12 us

profile of v2, /device:TPU:0, one launch (start us, length us, event | category | flops | bytes accessed | tf_op | source)
XLA Modules:
  0.0 130.7 jit_solution(15252363249664379694)
XLA Ops:
  0.6 126.9 %fused.1 = (bf16[1024,512]{1,0:T(8,128)(2,1)}, bf16[128,2048]{1,0:T(8,128)(2,1)}) custom-call(s32[2,512]{1,0:T(2,128)} %bitcast.18, f32[2,512]{1,0:T(2,128)} %bitcast.19, f32[1,256]{1,0:T(1,128)} %bitcast.20, f32[2,1024]{1,0:T(2,128)} %bitcast.15, f32[1,256]{1,0:T(1,128)} %bitcast.21, f32[1,2048]{1,0:T(1,128)} %bitcast.16, f32[1,2048]{1,0:T(1,128)} %bitcast.17, ...), custom_call_target="tpu_custom_call" | custom-call | tf_op jit(solution)/shard_map/fused/pallas_call | solution.py:689
  127.6 0.0 copy-start
  127.6 2.3 %copy.20 = bf16[1024,512]{1,0:T(8,128)(2,1)} copy(bf16[1024,512]{1,0:T(8,128)(2,1)} %get-tuple-element.4) | data formatting | bytes 2097152
  129.9 0.0 copy-done
  129.9 0.8 copy.21
Async XLA Ops:
  127.6 2.3 %copy-start = (bf16[128,2048]{1,0:T(8,128)(2,1)S(1)}, bf16[128,2048]{1,0:T(8,128)(2,1)}, u32[]{:S(2)}) copy-start(bf16[128,2048]{1,0:T(8,128)(2,1)} %get-tuple-element.5) | copy-start | bytes 1572868

commit v3 on v2

--- a/solution.py
+++ b/solution.py
@@ -14,6 +14,7 @@
 PIECES = 4
 STEP = 512
 TILE = 16
+LIMIT = 62
 
 NORM_EPS = 1e-06
 SWISH_ALPHA = 1.702
@@ -84,14 +85,15 @@
 
 
 def kernel(
-    n, planes, capacity, experts, named_by, shared_by, margin, extra, scale, lead, trail,
-    tok_hbm, probe_hbm, ret_hbm, val_hbm, switch_hbm, mix_hbm, gate_hbm, up_hbm, down_hbm,
+    n, planes, capacity, experts,
+    named_hbm, shared_hbm, margin_hbm, extra_hbm, scale_hbm, lead_hbm, trail_hbm, tok_hbm, probe_hbm, ret_hbm, val_hbm, switch_hbm, mix_hbm, gate_hbm, up_hbm, down_hbm,
+    mix_hbm_out, moe_hbm_out,
     mix_out, moe_out,
-    nt, probe, ret, val, switch, mix_w, gate_w, up_w, down_w,
-    rk, sh, meta, relay, meta2, relay2, rows, part, acc, sendb, recvb, fin, back, pk, pk2, pko, comb, spread,
+    named_by, shared_by, margin, extra, scale, lead, trail, nt, probe, ret, val, switch, mix_w, gate_w, up_w, down_w,
+    rk, sh, meta, relay, meta2, relay2, rows, part, acc, sendb, recvb, back, pk, pk2, pko, comb, spread, share_hi, share_lo,
     raw, qdec, state, state_bf, running, plst, pld, chain_in, chain_out, enter, carry, gath,
-    load_sem,
-    fsend, frecv, msend, mrecv, ysend, yrecv, zsend, zrecv, tsend, trecv, vsend, vrecv,
+    load_sem, store_sem, moe_sem,
+    fsend, frecv, msend, mrecv, ysend, yrecv, zsend, zrecv, tsend, trecv, vsend, vrecv, qsend, qrecv,
     xsend, xrecv, csend, crecv, dsend, drecv,
     esend0, erecv0, esend1, erecv1, bsend, brecv, rsend, rrecv,
     pssend, psrecv, pdsend, pdrecv, chsend, chrecv,
@@ -110,9 +112,11 @@
     f32, bf = jnp.float32, jnp.bfloat16
 
     pairs = (
-        (tok_hbm, nt), (probe_hbm, probe), (ret_hbm, ret), (val_hbm, val),
+        (tok_hbm, nt), (lead_hbm, lead), (named_hbm, named_by), (shared_hbm, shared_by),
+        (margin_hbm, margin), (extra_hbm, extra),
+        (probe_hbm, probe), (ret_hbm, ret), (val_hbm, val),
         (gate_hbm, gate_w), (up_hbm, up_w), (down_hbm, down_w),
-        (switch_hbm, switch), (mix_hbm, mix_w),
+        (switch_hbm, switch), (mix_hbm, mix_w), (scale_hbm, scale), (trail_hbm, trail),
     )
     loads = [pltpu.make_async_copy(a, b, load_sem.at[w]) for w, (a, b) in enumerate(pairs)]
     for load in loads:
@@ -127,6 +131,13 @@
     lax.fori_loop(1, n, hello, 0)
     for t in (mate, cross):
         pl.semaphore_signal(barrier, inc=1, device_id=(i, t), device_id_type=MESH)
+    for r in range(1, group):
+        d = p * group + (g + r) % group
+        pl.semaphore_signal(barrier, inc=1, device_id=(d, cross), device_id_type=MESH)
+
+    more = (p + planes - 1) // planes
+    less = (2 * planes - 2 - p) // planes
+    early = more * less
 
     def plane(s):
         left, right = p, planes - 1 - p
@@ -140,12 +151,25 @@
         other = (s + planes - 1) // planes - s // planes
         return p + other * sign * far
 
+    half = max(group // 2, 1)
+
+    def table(h, values):
+        total = values[0]
+        for v in range(1, len(values)):
+            total = total + (values[v] - values[v - 1]) * ((h + len(values) - v) // len(values))
+        return total
+
     def place(c):
-        t = (c + 1) // group
-        last = (t + 1) // planes
-        s = t + (t + planes - 1) // planes - last * (planes - 1)
+        away = (c + 1 - group + n) // n
+        rest = away * (c + 1 - group)
+        h = rest // half
+        inside = (table(h, (2, 2, 3, 3, 1, 1)), table(h, (0, 0, 2, 2, 4, 4)))
+        outside = (table(h, (2, 2, 1, 3, 3, 1)), table(h, (0, 0, 2, 3, 3, 4)))
+        s, base = (early * a + (1 - early) * b for a, b in zip(inside, outside))
+        s = away * s
+        r = away * (rest - half * base) + (1 - away) * (c + 1)
         q = plane(s)
-        return s, q, q * group + (g + (c + 1) % group) % group
+        return s, r, q * group + (g + r) % group
 
     def ranks():
         ids = lax.broadcasted_iota(jnp.int32, (experts, TOK_DEV), 0)
@@ -209,6 +233,14 @@
     def got_y(k):
         return remote(pk.at[0, 0], rows.at[k, j], ysend.at[0, 0], yrecv.at[k], (i, mate))
 
+    def over_xy(q, r):
+        k = q * group + g
+        d = p * group + (g + r) % group
+        return remote(pk.at[q, r - 1], rows.at[k, j], qsend.at[q, r], qrecv.at[k], (d, cross))
+
+    def got_xy(k):
+        return remote(pk.at[0, 0], rows.at[k, cross], qsend.at[0, 0], qrecv.at[k], (i, mate))
+
     def near(r, w):
         d = p * group + (g + r) % group
         b = (j, cross)[w]
@@ -238,20 +270,51 @@
         return remote(sendb.at[k], recvb.at[k], bsend.at[k], brecv.at[k], (i, cross))
 
     def home(k):
-        return remote(fin.at[k], back.at[i], rsend.at[k], rrecv.at[i], (k, j))
+        return remote(sendb.at[k], back.at[i], rsend.at[k], rrecv.at[i], (k, j))
 
     def home_in(k):
-        return remote(fin.at[k], back.at[k], rsend.at[k], rrecv.at[k], (k, j))
-
-    def twin():
-        q = plane(1)
-        return (
-            remote(nt.at[cross], relay2, tsend.at[0], trecv.at[0], (q * group + g, j)),
-            remote(rk.at[cross], meta2, tsend.at[1], trecv.at[1], (q * group + g, j)),
-        )
+        return remote(sendb.at[k], back.at[k], rsend.at[k], rrecv.at[k], (k, j))
+
+    upper = 2 * p // planes
+    source = (planes - 1) * (1 - upper)
+
+    def twin(side, first):
+        src = (nt.at[cross], rk.at[cross]) if first else (relay2.at[side], meta2.at[side])
+        dst = (relay2.at[side], meta2.at[side])
+        d = i + group - 2 * group * side
+        return [
+            remote(src[w], dst[w], tsend.at[side, w], trecv.at[side, w], (d, j)) for w in range(2)
+        ]
+
+    def twin_start():
+        @pl.when(p == 0)
+        def _():
+            for copy in twin(0, True):
+                copy.start()
+
+        @pl.when(p == planes - 1)
+        def _():
+            for copy in twin(1, True):
+                copy.start()
+
+    def twin_pass(side, used):
+        mine = (upper == 1) if side == 0 else (upper == 0)
+        take = mine if used else jnp.logical_not(mine)
+        reach = (p > 0) if side == 0 else (p < planes - 1)
+        on = (p < planes - 1) if side == 0 else (p > 0)
+
+        @pl.when(take & reach)
+        def _():
+            for copy in twin(side, False):
+                copy.wait_recv()
+
+        @pl.when(take & reach & on)
+        def _():
+            for copy in twin(side, False):
+                copy.start()
 
     def twin_y(r):
-        k = plane(1) * group + g
+        k = source * group + g
         d = p * group + (g + r) % group
         return remote(pk2.at[r - 1], rows.at[k, cross], vsend.at[r], vrecv.at[k], (d, j))
 
@@ -277,6 +340,17 @@
         def _():
             for copy in step_left(q, relay.at[q], meta.at[q]):
                 copy.start()
+
+    def direct(s):
+        return (s >= 1) & (s < planes - 1) & (s > early)
+
+    def late():
+        q = plane(1)
+        over_x(q * group + g).start()
+        for r in range(1, group):
+            k = q * group + (g + r) % group
+            got_y(k).wait_recv()
+            over_x(k).start()
 
     def arrive(s):
         q = plane(s)
@@ -289,40 +363,27 @@
 
         pack(meta.at[q], relay.at[q], rows.at[k, j], pk.at[q])
 
-        @pl.when(s >= 2)
+        @pl.when(direct(s))
         def _():
             over_x(k).start()
-
-        over_c(k).start()
+            for r in range(1, group):
+                over_xy(q, r).start()
+
         for r in range(1, group):
             over_y(q, r).start()
 
-    def arrive_y(s):
-        q = plane(s)
-        for r in range(1, group):
-            k = q * group + (g + r) % group
-            got_y(k).wait_recv()
-
-            @pl.when(s >= 2)
+    def arrive_twin():
+        k = source * group + g
+        for side in range(2):
+            twin_pass(side, True)
+        for side in range(2):
+
+            @pl.when(upper == 1 - side)
             def _():
-                over_x(k).start()
-
-            over_c(k).start()
-
-    def arrive_twin():
-        k = plane(1) * group + g
-        for copy in twin():
-            copy.wait_recv()
-        pack(meta2, relay2, rows.at[k, cross], pk2)
-        over_d(k).start()
+                pack(meta2.at[side], relay2.at[side], rows.at[k, cross], pk2)
+
         for r in range(1, group):
             twin_y(r).start()
-
-    def arrive_twin_y():
-        for r in range(1, group):
-            k = plane(1) * group + (g + r) % group
-            got_twin_y(k).wait_recv()
-            over_d(k).start()
 
     def expert(k):
         x = rows[k].reshape(4 * capacity, features)
@@ -335,12 +396,34 @@
         to_mate(k, False).start()
         to_mate(k, True).start()
 
-    def work(k, s):
-        @pl.when(s >= 2)
+    def prepare(c):
+        s, r, k = place(c)
+
+        @pl.when(s == 0)
+        def _():
+            got_near(k, 0).wait_recv()
+            got_near(k, 1).wait_recv()
+
+        @pl.when((r >= 1) & (direct(s) | ((s >= 1) & (s == planes - 1))))
+        def _():
+            got_y(k).wait_recv()
+
+        @pl.when((s >= 1) & (s == planes - 1) & (r >= 1))
+        def _():
+            got_twin_y(k).wait_recv()
+
+        @pl.when(direct(s) & (r >= 1))
+        def _():
+            got_xy(k).wait_recv()
+
+        @pl.when((s >= 1) & (s < planes - 1) & ((r == 0) | (s <= early)))
         def _():
             over_x(k).wait_recv()
-            over_d(k).start()
-
+
+        over_c(k).start()
+        over_d(k).start()
+
+    def work(k):
         over_c(k).wait_recv()
         over_d(k).wait_recv()
         expert(k)
@@ -418,6 +501,9 @@
     def mix_d(c):
         here = gath.at[cross, at(c)]
         return remote(here, here, gdsend.at[c], gdrecv.at[c], (i, mate))
+
+    def store(c):
+        return pltpu.make_async_copy(mix_out.at[at(c)], mix_hbm_out.at[at(c)], store_sem.at[c])
 
     def mix_final(c, z):
         r = at(c)
@@ -448,12 +534,16 @@
                 gath[w, r, :], mix_w[w * width : (w + 1) * width, :], preferred_element_type=f32
             )
         mix_out[r, :] = a.astype(bf)
+        store(c).start()
         return z
 
+    for load in loads[2:4]:
+        load.wait()
     ranks()
-    loads[0].wait()
+    for load in loads[:2]:
+        load.wait()
     norm(j)
-    pl.semaphore_wait(barrier, n + 1)
+    pl.semaphore_wait(barrier, n + group)
 
     @pl.when(p + 1 < planes)
     def _():
@@ -466,6 +556,8 @@
             copy.start()
 
     norm(cross)
+    if planes > 1:
+        twin_start()
     for w, b in enumerate((j, cross)):
         pack(rk.at[b], nt.at[b], rows.at[i, b], pko.at[w])
         for r in range(1, group):
@@ -475,7 +567,7 @@
     for b in (mate, mate_cross):
         pack(rk.at[b], nt.at[b], rows.at[i, b], None)
 
-    for load in loads[1:4]:
+    for load in loads[4:9]:
         load.wait()
     state[...] = jnp.zeros_like(state)
     running[...] = jnp.zeros_like(running)
@@ -484,15 +576,11 @@
         span_step(t, probe, ret, val, margin, extra, raw, qdec, state, running)
         return c
 
-    half = length // SPAN // 2
-    for load in loads[4:]:
+    for load in loads[9:]:
         load.wait()
     expert(i)
     first_sum(i)
-    lax.fori_loop(0, half, spans, 0)
-    if planes > 1:
-        forward(1)
-    lax.fori_loop(half, length // SPAN, spans, 0)
+    lax.fori_loop(0, length // SPAN, spans, 0)
     for h in range(heads):
         state_bf[h] = state[h].astype(bf)
     plst[g] = state_bf[...]
@@ -500,68 +588,96 @@
     for r in range(1, group):
         for copy in in_plane(r):
             copy.start()
-    for r in range(1, group):
-        k = p * group + (g + r) % group
-        got_near(k, 0).wait_recv()
-        over_c(k).start()
-        got_near(k, 1).wait_recv()
-        over_d(k).start()
+    for t in range(1, min(planes, 3)):
+        forward(t)
+
+    if planes > 1:
+        @pl.when(early > 0)
+        def _():
+            arrive(2)
+
+        arrive(1)
+    prepare(0)
 
     def turn(u):
-        return u - (u + n - group) // n
+        return u - (1 - early) * ((u + n - group) // n)
+
+    def busy(u):
+        return (u >= 0) & (u < n - early) & ((early > 0) | (u != group - 1))
+
+    def ready(u):
+        @pl.when(busy(u))
+        def _():
+            prepare(turn(u))
 
     def pump(u, z):
-        @pl.when(u < planes - 2)
+        @pl.when((u >= 1) & (u < planes - 2))
         def _():
             forward(u + 2)
 
         @pl.when(u == 1)
         def _():
-            for copy in twin():
-                copy.start()
-
-        @pl.when((u < n) & (u != group - 1))
-        def _():
-            s, q, k = place(turn(u))
-            work(k, s)
+            for side in range(2):
+                twin_pass(side, False)
+
+        @pl.when(busy(u))
+        def _():
+            s, r, k = place(turn(u))
+            work(k)
             first_sum(k)
 
-        @pl.when(u < planes - 1)
-        def _():
-            arrive(u + 1)
-
-        @pl.when((u >= 1) & (u < n + 1) & (u != group))
-        def _():
-            s, q, k = place(turn(u - 1))
-            fin[k] = total(k)
+        @pl.when(u == n - 1 - early)
+        def _():
+            lax.fori_loop(0, PIECES, mix_final, 0)
+
+        if planes > 1:
+
+            @pl.when((u == 1) | (u == 2 - early))
+            def _():
+                arrive(u + 1 + early)
+
+            @pl.when(u == 12 * early - 9)
+            def _():
+                late()
+
+        if planes > 1:
+
+            @pl.when(u == 3 - early)
+            def _():
+                arrive_twin()
+
+        @pl.when(u >= planes)
+        def _():
+            ready(u + 1)
+
+        @pl.when(busy(u - 1))
+        def _():
+            s, r, k = place(turn(u - 1))
+            sendb[k] = total(k)
             home(k).start()
 
         @pl.when(u == 0)
         def _():
             back[i] = total(i)
+            weights()
+
+        @pl.when(u == p)
+        def _():
             prefix()
 
-        @pl.when(u < planes - 1)
-        def _():
-            arrive_y(u + 1)
-
-        @pl.when(u == planes)
-        def _():
-            arrive_twin()
-
-        @pl.when(u == planes + 1)
-        def _():
-            arrive_twin_y()
-
-        @pl.when(u == n - 1)
-        def _():
-            lax.fori_loop(0, PIECES, mix_final, 0)
+        @pl.when(u < planes)
+        def _():
+            ready(u + 1)
 
         return z
 
-    lax.fori_loop(0, n + 1, pump, 0)
-    lax.fori_loop(0, PIECES, mix_pass, 0)
-    lax.fori_loop(0, PIECES, mix_project, 0)
+    def weights():
+        lax.fori_loop(0, experts, weigh, 0)
+        for b in range(n * capacity // TOK_DEV):
+            wide = jnp.transpose(spread[b * TOK_DEV : (b + 1) * TOK_DEV, :])
+            high = wide.astype(bf)
+            share_hi[b] = high
+            share_lo[b] = (wide - high.astype(f32)).astype(bf)
 
     def weigh(e, z):
         r = pl.ds(pl.multiple_of(e * capacity, capacity), capacity)
@@ -570,22 +686,26 @@
         )
         return z
 
-    lax.fori_loop(0, experts, weigh, 0)
-    wide = spread[...]
-    high = wide.astype(bf)
-    low = (wide - high.astype(f32)).astype(bf)
-
-    def collect(s, z):
-        k = (i + s) % n
-        home_in(k).wait_recv()
-        return z
-
-    lax.fori_loop(1, n, collect, 0)
-    for f in range(0, features, STEP):
-        flat = back[:, :, f : f + STEP].reshape(n * capacity, STEP)
-        comb[:, f : f + STEP] = lax.dot_general(
-            high, flat, TN, preferred_element_type=f32
-        ) + lax.dot_general(low, flat, TN, preferred_element_type=f32)
+    lax.fori_loop(0, n + 1, pump, 0)
+    lax.fori_loop(0, PIECES, mix_pass, 0)
+    lax.fori_loop(0, PIECES, mix_project, 0)
+
+    def collect(s, first):
+        q = plane(s)
+        for r in range(group):
+            k = q * group + (g + r) % group
+            if not (first and r == 0):
+                home_in(k).wait_recv()
+        for f in range(0, features, STEP):
+            flat = back[pl.ds(q * group, group), :, f : f + STEP].reshape(group * capacity, STEP)
+            y = jnp.dot(share_hi[q], flat, preferred_element_type=f32) + jnp.dot(
+                share_lo[q], flat, preferred_element_type=f32
+            )
+            comb[:, f : f + STEP] = y if first else comb[:, f : f + STEP] + y
+
+    collect(0, True)
+    for s in range(1, planes):
+        collect(s, False)
 
     def closing(t, z):
         r = pl.ds(pl.multiple_of(t * TILE, TILE), TILE)
@@ -593,6 +713,8 @@
         return z
 
     lax.fori_loop(0, TOK_DEV // TILE, closing, 0)
+    last = pltpu.make_async_copy(moe_out, moe_hbm_out, moe_sem)
+    last.start()
 
     def finish(s, z):
         k = (i + s) % n
@@ -606,10 +728,19 @@
     def finish_far(s, z):
         q = plane(s)
 
-        @pl.when(s >= 2)
-        def _():
-            for r in range(group):
-                over_x(q * group + r).wait_send()
+        @pl.when(s < planes - 1)
+        def _():
+            over_x(q * group + g).wait_send()
+
+        @pl.when(s <= early)
+        def _():
+            for r in range(1, group):
+                over_x(q * group + (g + r) % group).wait_send()
+
+        @pl.when(direct(s))
+        def _():
+            for r in range(1, group):
+                over_xy(q, r).wait_send()
 
         for r in range(1, group):
             over_y(q, r).wait_send()
@@ -640,8 +771,13 @@
             copy.wait_send()
 
     if planes > 1:
-        for copy in twin():
-            copy.wait_send()
+        for side in range(2):
+
+            @pl.when((p < planes - 1) if side == 0 else (p > 0))
+            def _():
+                for copy in twin(side, False):
+                    copy.wait_send()
+
         for r in range(1, group):
             twin_y(r).wait_send()
     for r in range(1, group):
@@ -649,6 +785,9 @@
             near(r, w).wait_send()
         for copy in in_plane(r):
             copy.wait_send()
+    for c in range(PIECES):
+        store(c).wait()
+    last.wait()
 
 
 def shards(
@@ -673,7 +812,7 @@
     experts = specialist_switch_matrix.shape[0] * n
     top_count = specialist_assignment.shape[1]
     capacity = 2 * TOK_DEV * top_count // experts
-    planes = max(d for d in (1, 2, STAGES) if n % (2 * d) == 0)
+    planes = STAGES if n % (2 * STAGES) == 0 else 1
     group = n // planes
     length, width = state_probe_logits.shape
     heads = width // HEAD
@@ -681,8 +820,7 @@
     hidden = specialist_switch_matrix.shape[2]
     columns = state_result_matrix.shape[1]
     bf, f32 = jnp.bfloat16, jnp.float32
-    vm = pl.BlockSpec(memory_space=VMEM)
-    hbm = pl.BlockSpec(memory_space=pl.ANY)
+    hbm = pl.BlockSpec(memory_space=pltpu.HBM)
     chunk = (capacity, features)
     block = (TOK_DEV, features)
     return tuple(
@@ -693,9 +831,18 @@
                 jax.ShapeDtypeStruct((length, columns), bf),
                 jax.ShapeDtypeStruct(block, bf),
             ),
-            in_specs=[vm] * 7 + [hbm] * 9,
-            out_specs=(vm, vm),
+            in_specs=[hbm] * 16,
+            out_specs=(hbm, hbm),
             scratch_shapes=[
+                VMEM((length, columns), bf),
+                VMEM(block, bf),
+                VMEM((top_count, 4 * TOK_DEV), jnp.int32),
+                VMEM((top_count, 4 * TOK_DEV), f32),
+                VMEM((1, width), f32),
+                VMEM((heads, length), f32),
+                VMEM((1, width), f32),
+                VMEM((1, features), f32),
+                VMEM((1, features), f32),
                 VMEM((4,) + block, bf),
                 VMEM((length, width), bf),
                 VMEM((length, width), bf),
@@ -709,12 +856,11 @@
                 VMEM((4, experts, TOK_DEV), f32),
                 VMEM((planes, experts, TOK_DEV), f32),
                 VMEM((planes,) + block, bf),
-                VMEM((experts, TOK_DEV), f32),
-                VMEM(block, bf),
+                VMEM((2, experts, TOK_DEV), f32),
+                VMEM((2,) + block, bf),
                 VMEM((n, 4) + chunk, bf),
                 VMEM((n, 4) + chunk, bf),
                 VMEM((2, n) + chunk, bf),
-                VMEM((n,) + chunk, bf),
                 VMEM((n,) + chunk, bf),
                 VMEM((n,) + chunk, bf),
                 VMEM((n,) + chunk, bf),
@@ -723,6 +869,8 @@
                 VMEM((2, group - 1) + chunk, bf),
                 VMEM(block, f32),
                 VMEM((n * capacity, TOK_DEV), f32),
+                VMEM((planes, TOK_DEV, TOK_DEV), bf),
+                VMEM((planes, TOK_DEV, TOK_DEV), bf),
                 VMEM((length, width), f32),
                 VMEM((length, width), bf),
                 VMEM((heads, HEAD, HEAD), f32),
@@ -735,17 +883,18 @@
                 VMEM((heads, HEAD, HEAD), f32),
                 VMEM((heads, HEAD, HEAD), f32),
                 VMEM((4, length, width), bf),
-                DMA((9,)),
+                DMA((16,)), DMA((PIECES,)), DMA,
                 DMA((2, planes)), DMA((planes,)), DMA((2, planes)), DMA((planes,)),
                 DMA((planes, group)), DMA((n,)), DMA((2, group)), DMA((2, n)),
-                DMA((2,)), DMA((2,)), DMA((group,)), DMA((n,)),
+                DMA((2, 2)), DMA((2, 2)), DMA((group,)), DMA((n,)),
+                DMA((planes, group)), DMA((n,)),
             ]
             + [DMA((n,))] * 14
             + [DMA((group,))] * 4
             + [DMA, DMA]
             + [DMA((PIECES,))] * 6,
             compiler_params=pltpu.CompilerParams(
-                collective_id=0, has_side_effects=True, vmem_limit_bytes=62 * 2**20
+                collective_id=0, has_side_effects=True, vmem_limit_bytes=LIMIT * 2**20
             ),
         )(
             specialist_assignment.T,

time: 131 us -> 117 us (0.89)
  Pallas kernels: 127 us -> 113 us
    pallas_call x1, Pallas kernels: 127 us -> 113 us  [shards(): pl.pallas_call(functools.partial(kernel, n, planes, capacity, experts), n...]
where the time goes in v3:
time: 117 us
  Pallas kernels  113 us (97%)
  local copies, waits for them, and re-layouts  3.12 us (3%)
    pallas_call x1, Pallas kernels, shards(): pl.pallas_call(functools.partial(kernel, n, planes, capacity, experts), n...  113 us
    unnamed x4, local copies, waits for them, and re-layouts  3.12 us

profile of v3, /device:TPU:0, one launch (start us, length us, event | category | flops | bytes accessed | tf_op | source)
XLA Modules:
  0.0 116.5 jit_solution(17359403544278641347)
XLA Ops:
  0.6 112.8 %fused.1 = (bf16[1024,512]{1,0:T(8,128)(2,1)}, bf16[128,2048]{1,0:T(8,128)(2,1)}) custom-call(s32[2,512]{1,0:T(2,128)} %bitcast.18, f32[2,512]{1,0:T(2,128)} %bitcast.19, f32[1,256]{1,0:T(1,128)} %bitcast.20, f32[2,1024]{1,0:T(2,128)} %bitcast.15, f32[1,256]{1,0:T(1,128)} %bitcast.21, f32[1,2048]{1,0:T(1,128)} %bitcast.16, f32[1,2048]{1,0:T(1,128)} %bitcast.17, ...), custom_call_target="tpu_custom_call" | custom-call | tf_op jit(solution)/shard_map/fused/pallas_call | solution.py:827
  113.4 0.0 copy-start
  113.4 2.3 %copy.20 = bf16[1024,512]{1,0:T(8,128)(2,1)} copy(bf16[1024,512]{1,0:T(8,128)(2,1)} %get-tuple-element.4) | data formatting | bytes 2097152
  115.7 0.0 copy-done
  115.7 0.8 copy.21
Async XLA Ops:
  113.4 2.3 %copy-start = (bf16[128,2048]{1,0:T(8,128)(2,1)S(1)}, bf16[128,2048]{1,0:T(8,128)(2,1)}, u32[]{:S(2)}) copy-start(bf16[128,2048]{1,0:T(8,128)(2,1)} %get-tuple-element.5) | copy-start | bytes 1572868

commit v4 on v3

--- a/solution.py
+++ b/solution.py
@@ -90,7 +90,7 @@
     mix_hbm_out, moe_hbm_out,
     mix_out, moe_out,
     named_by, shared_by, margin, extra, scale, lead, trail, nt, probe, ret, val, switch, mix_w, gate_w, up_w, down_w,
-    rk, sh, meta, relay, meta2, relay2, rows, part, acc, sendb, recvb, back, pk, pk2, pko, comb, spread, share_hi, share_lo,
+    act, rk, sh, meta, relay, meta2, relay2, rows, part, acc, sendb, recvb, back, pk, pk2, pko, comb, spread, share_hi, share_lo,
     raw, qdec, state, state_bf, running, plst, pld, chain_in, chain_out, enter, carry, gath,
     load_sem, store_sem, moe_sem,
     fsend, frecv, msend, mrecv, ysend, yrecv, zsend, zrecv, tsend, trecv, vsend, vrecv, qsend, qrecv,
@@ -345,8 +345,10 @@
         return (s >= 1) & (s < planes - 1) & (s > early)
 
     def late():
+        over_x(plane(1) * group + g).start()
+
+    def later():
         q = plane(1)
-        over_x(q * group + g).start()
         for r in range(1, group):
             k = q * group + (g + r) % group
             got_y(k).wait_recv()
@@ -366,11 +368,14 @@
         @pl.when(direct(s))
         def _():
             over_x(k).start()
+
+        for r in range(1, group):
+            over_y(q, r).start()
+
+        @pl.when(direct(s))
+        def _():
             for r in range(1, group):
                 over_xy(q, r).start()
-
-        for r in range(1, group):
-            over_y(q, r).start()
 
     def arrive_twin():
         k = source * group + g
@@ -389,12 +394,16 @@
         x = rows[k].reshape(4 * capacity, features)
         gate = jnp.dot(x, gate_w[...], preferred_element_type=f32)
         upward = jnp.dot(x, up_w[...], preferred_element_type=f32)
-        act = clamped_unit(gate, upward).astype(bf)
-        for f in range(0, features, STEP):
-            y = jnp.dot(act, down_w[:, f : f + STEP], preferred_element_type=f32)
-            part[k, :, :, f : f + STEP] = y.astype(bf).reshape(4, capacity, STEP)
-        to_mate(k, False).start()
-        to_mate(k, True).start()
+        act[...] = clamped_unit(gate, upward).astype(bf).reshape(act.shape)
+        for one, two in ((mate_cross, mate), (cross, j)):
+            a = jnp.concatenate([act[one], act[two]], axis=0)
+            for f in range(0, features, STEP):
+                y = jnp.dot(a, down_w[:, f : f + STEP], preferred_element_type=f32).astype(bf)
+                part[k, one, :, f : f + STEP] = y[:capacity]
+                part[k, two, :, f : f + STEP] = y[capacity:]
+            if one is mate_cross:
+                to_mate(k, False).start()
+                to_mate(k, True).start()
 
     def prepare(c):
         s, r, k = place(c)
@@ -432,7 +441,6 @@
         to_mate(k, False).wait()
         x = part[k, cross].astype(f32) + acc[1, k].astype(f32)
         sendb[k] = x.astype(bf)
-        to_cross(k).start()
 
     def total(k):
         to_mate(k, True).wait()
@@ -580,6 +588,7 @@
         load.wait()
     expert(i)
     first_sum(i)
+    to_cross(i).start()
     lax.fori_loop(0, length // SPAN, spans, 0)
     for h in range(heads):
         state_bf[h] = state[h].astype(bf)
@@ -626,6 +635,16 @@
             work(k)
             first_sum(k)
 
+            @pl.when((early > 0) | (u >= group))
+            def _():
+                to_cross(k).start()
+
+        @pl.when((early == 0) & (u == group + 1))
+        def _():
+            for c in range(group - 1):
+                s, r, k = place(c)
+                to_cross(k).start()
+
         @pl.when(u == n - 1 - early)
         def _():
             lax.fori_loop(0, PIECES, mix_final, 0)
@@ -636,26 +655,37 @@
             def _():
                 arrive(u + 1 + early)
 
-            @pl.when(u == 12 * early - 9)
+            @pl.when((early > 0) & (u == 2))
             def _():
                 late()
 
+            @pl.when((early > 0) & (u == 3))
+            def _():
+                later()
+
         if planes > 1:
 
-            @pl.when(u == 3 - early)
+            @pl.when(u == 4 - 2 * early)
             def _():
                 arrive_twin()
 
-        @pl.when(u >= planes)
+        @pl.when((u >= planes) & (early == 0))
         def _():
             ready(u + 1)
 
-        @pl.when(busy(u - 1))
+        @pl.when(busy(u - 1) & (u >= group + 1 - early))
         def _():
             s, r, k = place(turn(u - 1))
             sendb[k] = total(k)
             home(k).start()
 
+        @pl.when(u == n - 2)
+        def _():
+            for c in range(group - 1):
+                s, r, k = place(c)
+                sendb[k] = total(k)
+                home(k).start()
+
         @pl.when(u == 0)
         def _():
             back[i] = total(i)
@@ -665,7 +695,7 @@
         def _():
             prefix()
 
-        @pl.when(u < planes)
+        @pl.when((u < planes) | (early > 0))
         def _():
             ready(u + 1)
 
@@ -687,14 +717,87 @@
         return z
 
     lax.fori_loop(0, n + 1, pump, 0)
-    lax.fori_loop(0, PIECES, mix_pass, 0)
-    lax.fori_loop(0, PIECES, mix_project, 0)
-
+    def mix_both(c, z):
+        mix_pass(c, z)
+        return mix_project(c - 1, z)
+
+    mix_pass(0, 0)
+    lax.fori_loop(1, PIECES, mix_both, 0)
+    mix_project(PIECES - 1, 0)
+
+    def finish(s, z):
+        k = (i + s) % n
+        over_c(k).wait_send()
+        over_d(k).wait_send()
+        return z
+
+    lax.fori_loop(1, n, finish, 0)
+
+    def finish_far(s, z):
+        q = plane(s)
+
+        @pl.when(s < planes - 1)
+        def _():
+            over_x(q * group + g).wait_send()
+
+        @pl.when(s <= early)
+        def _():
+            for r in range(1, group):
+                over_x(q * group + (g + r) % group).wait_send()
+
+        @pl.when(direct(s))
+        def _():
+            for r in range(1, group):
+                over_xy(q, r).wait_send()
+
+        for r in range(1, group):
+            over_y(q, r).wait_send()
+
+        @pl.when((q < p) & (p + 1 < planes))
+        def _():
+            for copy in step_right(q, relay.at[q], meta.at[q]):
+                copy.wait_send()
+
+        @pl.when((q > p) & (p >= 1))
+        def _():
+            for copy in step_left(q, relay.at[q], meta.at[q]):
+                copy.wait_send()
+
+        return z
+
+    lax.fori_loop(1, planes, finish_far, 0)
+
+    @pl.when(p + 1 < planes)
+    def _():
+        for copy in step_right(p, nt.at[j], rk.at[j]):
+            copy.wait_send()
+        chain().wait_send()
+
+    @pl.when(p >= 1)
+    def _():
+        for copy in step_left(p, nt.at[j], rk.at[j]):
+            copy.wait_send()
+
+    if planes > 1:
+        for side in range(2):
+
+            @pl.when((p < planes - 1) if side == 0 else (p > 0))
+            def _():
+                for copy in twin(side, False):
+                    copy.wait_send()
+
+        for r in range(1, group):
+            twin_y(r).wait_send()
+    for r in range(1, group):
+        for w in range(2):
+            near(r, w).wait_send()
+        for copy in in_plane(r):
+            copy.wait_send()
     def collect(s, first):
         q = plane(s)
         for r in range(group):
             k = q * group + (g + r) % group
-            if not (first and r == 0):
+            if s > 0 or r > 0:
                 home_in(k).wait_recv()
         for f in range(0, features, STEP):
             flat = back[pl.ds(q * group, group), :, f : f + STEP].reshape(group * capacity, STEP)
@@ -703,91 +806,36 @@
             )
             comb[:, f : f + STEP] = y if first else comb[:, f : f + STEP] + y
 
-    collect(0, True)
-    for s in range(1, planes):
-        collect(s, False)
+    turns = [2, 3, 0, 1] if planes > 1 else [0]
+    for s in turns:
+        collect(s, s == turns[0])
 
     def closing(t, z):
         r = pl.ds(pl.multiple_of(t * TILE, TILE), TILE)
         moe_out[r, :] = rms_scale(comb[r, :], trail[...]).astype(bf)
         return z
 
-    lax.fori_loop(0, TOK_DEV // TILE, closing, 0)
-    last = pltpu.make_async_copy(moe_out, moe_hbm_out, moe_sem)
-    last.start()
-
-    def finish(s, z):
-        k = (i + s) % n
-        over_c(k).wait_send()
-        over_d(k).wait_send()
-        home(k).wait_send()
+    quarter = TOK_DEV // PIECES
+
+    def last(c):
+        r = pl.ds(pl.multiple_of(c * quarter, quarter), quarter)
+        return pltpu.make_async_copy(moe_out.at[r], moe_hbm_out.at[r], moe_sem.at[c])
+
+    def close(c, z):
+        lax.fori_loop(c * (quarter // TILE), (c + 1) * (quarter // TILE), closing, 0)
+        last(c).start()
         return z
 
-    lax.fori_loop(1, n, finish, 0)
-
-    def finish_far(s, z):
-        q = plane(s)
-
-        @pl.when(s < planes - 1)
-        def _():
-            over_x(q * group + g).wait_send()
-
-        @pl.when(s <= early)
-        def _():
-            for r in range(1, group):
-                over_x(q * group + (g + r) % group).wait_send()
-
-        @pl.when(direct(s))
-        def _():
-            for r in range(1, group):
-                over_xy(q, r).wait_send()
-
-        for r in range(1, group):
-            over_y(q, r).wait_send()
-
-        @pl.when((q < p) & (p + 1 < planes))
-        def _():
-            for copy in step_right(q, relay.at[q], meta.at[q]):
-                copy.wait_send()
-
-        @pl.when((q > p) & (p >= 1))
-        def _():
-            for copy in step_left(q, relay.at[q], meta.at[q]):
-                copy.wait_send()
-
+    lax.fori_loop(0, PIECES, close, 0)
+
+    def finish_home(s, z):
+        home((i + s) % n).wait_send()
         return z
 
-    lax.fori_loop(1, planes, finish_far, 0)
-
-    @pl.when(p + 1 < planes)
-    def _():
-        for copy in step_right(p, nt.at[j], rk.at[j]):
-            copy.wait_send()
-        chain().wait_send()
-
-    @pl.when(p >= 1)
-    def _():
-        for copy in step_left(p, nt.at[j], rk.at[j]):
-            copy.wait_send()
-
-    if planes > 1:
-        for side in range(2):
-
-            @pl.when((p < planes - 1) if side == 0 else (p > 0))
-            def _():
-                for copy in twin(side, False):
-                    copy.wait_send()
-
-        for r in range(1, group):
-            twin_y(r).wait_send()
-    for r in range(1, group):
-        for w in range(2):
-            near(r, w).wait_send()
-        for copy in in_plane(r):
-            copy.wait_send()
+    lax.fori_loop(1, n, finish_home, 0)
     for c in range(PIECES):
         store(c).wait()
-    last.wait()
+        last(c).wait()
 
 
 def shards(
@@ -852,6 +900,7 @@
                 VMEM((features, hidden), bf),
                 VMEM((features, hidden), bf),
                 VMEM((hidden, features), bf),
+                VMEM((4, capacity, hidden), bf),
                 VMEM((4, experts, TOK_DEV), f32),
                 VMEM((4, experts, TOK_DEV), f32),
                 VMEM((planes, experts, TOK_DEV), f32),
@@ -883,7 +932,7 @@
                 VMEM((heads, HEAD, HEAD), f32),
                 VMEM((heads, HEAD, HEAD), f32),
                 VMEM((4, length, width), bf),
-                DMA((16,)), DMA((PIECES,)), DMA,
+                DMA((16,)), DMA((PIECES,)), DMA((PIECES,)),
                 DMA((2, planes)), DMA((planes,)), DMA((2, planes)), DMA((planes,)),
                 DMA((planes, group)), DMA((n,)), DMA((2, group)), DMA((2, n)),
                 DMA((2, 2)), DMA((2, 2)), DMA((group,)), DMA((n,)),

time: 117 us -> 112 us (0.957)
  Pallas kernels: 113 us -> 108 us
    pallas_call x1, Pallas kernels: 113 us -> 108 us  [shards(): pl.pallas_call(functools.partial(kernel, n, planes, capacity, experts), n...]
where the time goes in v4:
time: 112 us
  Pallas kernels  108 us (96%)
  local copies, waits for them, and re-layouts  3.12 us (3%)
    pallas_call x1, Pallas kernels, shards(): pl.pallas_call(functools.partial(kernel, n, planes, capacity, experts), n...  108 us
    unnamed x4, local copies, waits for them, and re-layouts  3.12 us

profile of v4, /device:TPU:0, one launch (start us, length us, event | category | flops | bytes accessed | tf_op | source)
XLA Modules:
  0.0 112.3 jit_solution(7849846187440239400)
XLA Ops:
  0.6 108.5 %fused.1 = (bf16[1024,512]{1,0:T(8,128)(2,1)}, bf16[128,2048]{1,0:T(8,128)(2,1)}) custom-call(s32[2,512]{1,0:T(2,128)} %bitcast.18, f32[2,512]{1,0:T(2,128)} %bitcast.19, f32[1,256]{1,0:T(1,128)} %bitcast.20, f32[2,1024]{1,0:T(2,128)} %bitcast.15, f32[1,256]{1,0:T(1,128)} %bitcast.21, f32[1,2048]{1,0:T(1,128)} %bitcast.16, f32[1,2048]{1,0:T(1,128)} %bitcast.17, ...), custom_call_target="tpu_custom_call" | custom-call | tf_op jit(solution)/shard_map/fused/pallas_call | solution.py:875
  109.1 0.0 copy-start
  109.1 2.3 %copy.20 = bf16[1024,512]{1,0:T(8,128)(2,1)} copy(bf16[1024,512]{1,0:T(8,128)(2,1)} %get-tuple-element.4) | data formatting | bytes 2097152
  111.5 0.0 copy-done
  111.5 0.8 copy.21
Async XLA Ops:
  109.1 2.3 %copy-start = (bf16[128,2048]{1,0:T(8,128)(2,1)S(1)}, bf16[128,2048]{1,0:T(8,128)(2,1)}, u32[]{:S(2)}) copy-start(bf16[128,2048]{1,0:T(8,128)(2,1)} %get-tuple-element.5) | copy-start | bytes 1572868

commit v5 on v4

--- a/solution.py
+++ b/solution.py
@@ -163,7 +163,7 @@
         away = (c + 1 - group + n) // n
         rest = away * (c + 1 - group)
         h = rest // half
-        inside = (table(h, (2, 2, 3, 3, 1, 1)), table(h, (0, 0, 2, 2, 4, 4)))
+        inside = (table(h, (1, 1, 3, 3, 2, 2)), table(h, (0, 0, 2, 2, 4, 4)))
         outside = (table(h, (2, 2, 1, 3, 3, 1)), table(h, (0, 0, 2, 3, 3, 4)))
         s, base = (early * a + (1 - early) * b for a, b in zip(inside, outside))
         s = away * s
@@ -213,17 +213,25 @@
             for r in range(1, len(picks)):
                 others[r - 1, :, f : f + STEP] = y[r * capacity : (r + 1) * capacity]
 
+    part_rows = TOK_DEV // 2
+
+    def step(q, src, info, side):
+        d = i + group - 2 * group * side
+        rows_of = [pl.ds(h * part_rows, part_rows) for h in range(2)]
+        return [
+            remote(info, meta.at[q], msend.at[side, q], mrecv.at[q], (d, j))
+        ] + [
+            remote(
+                src.at[w], relay.at[q].at[w], fsend.at[side, q, h], frecv.at[q, h], (d, j)
+            )
+            for h, w in enumerate(rows_of)
+        ]
+
     def step_right(q, src, info):
-        return (
-            remote(src, relay.at[q], fsend.at[0, q], frecv.at[q], (i + group, j)),
-            remote(info, meta.at[q], msend.at[0, q], mrecv.at[q], (i + group, j)),
-        )
+        return step(q, src, info, 0)
 
     def step_left(q, src, info):
-        return (
-            remote(src, relay.at[q], fsend.at[1, q], frecv.at[q], (i - group, j)),
-            remote(info, meta.at[q], msend.at[1, q], mrecv.at[q], (i - group, j)),
-        )
+        return step(q, src, info, 1)
 
     def over_y(q, r):
         k = q * group + g
@@ -282,8 +290,12 @@
         src = (nt.at[cross], rk.at[cross]) if first else (relay2.at[side], meta2.at[side])
         dst = (relay2.at[side], meta2.at[side])
         d = i + group - 2 * group * side
+        src, dst = (
+            [v[1]] + [v[0].at[pl.ds(h * part_rows, part_rows)] for h in range(2)]
+            for v in (src, dst)
+        )
         return [
-            remote(src[w], dst[w], tsend.at[side, w], trecv.at[side, w], (d, j)) for w in range(2)
+            remote(src[w], dst[w], tsend.at[side, w], trecv.at[side, w], (d, j)) for w in range(3)
         ]
 
     def twin_start():
@@ -303,15 +315,17 @@
         reach = (p > 0) if side == 0 else (p < planes - 1)
         on = (p < planes - 1) if side == 0 else (p > 0)
 
-        @pl.when(take & reach)
-        def _():
-            for copy in twin(side, False):
-                copy.wait_recv()
-
-        @pl.when(take & reach & on)
-        def _():
-            for copy in twin(side, False):
-                copy.start()
+        for which in (slice(0, 2), slice(2, 3)):
+
+            @pl.when(take & reach)
+            def _():
+                for copy in twin(side, False)[which]:
+                    copy.wait_recv()
+
+            @pl.when(take & reach & on)
+            def _():
+                for copy in twin(side, False)[which]:
+                    copy.start()
 
     def twin_y(r):
         k = source * group + g
@@ -323,32 +337,33 @@
 
     inner = (p >= 1) & (p + 1 < planes)
 
-    def forward(s):
+    def forward(s, h):
         q = plane(s)
+        which = slice(0, 2) if h == 0 else slice(2, 3)
 
         @pl.when(inner)
         def _():
-            for copy in step_right(q, relay.at[q], meta.at[q]):
+            for copy in step_right(q, relay.at[q], meta.at[q])[which]:
                 copy.wait_recv()
 
         @pl.when(inner & (q < p))
         def _():
-            for copy in step_right(q, relay.at[q], meta.at[q]):
+            for copy in step_right(q, relay.at[q], meta.at[q])[which]:
                 copy.start()
 
         @pl.when(inner & (q > p))
         def _():
-            for copy in step_left(q, relay.at[q], meta.at[q]):
+            for copy in step_left(q, relay.at[q], meta.at[q])[which]:
                 copy.start()
 
     def direct(s):
-        return (s >= 1) & (s < planes - 1) & (s > early)
+        return (s >= 1) & (s < planes - 1) & (s != 2 * early)
 
     def late():
-        over_x(plane(1) * group + g).start()
+        over_x(plane(2) * group + g).start()
 
     def later():
-        q = plane(1)
+        q = plane(2)
         for r in range(1, group):
             k = q * group + (g + r) % group
             got_y(k).wait_recv()
@@ -425,7 +440,7 @@
         def _():
             got_xy(k).wait_recv()
 
-        @pl.when((s >= 1) & (s < planes - 1) & ((r == 0) | (s <= early)))
+        @pl.when((s >= 1) & (s < planes - 1) & ((r == 0) | (s == 2 * early)))
         def _():
             over_x(k).wait_recv()
 
@@ -589,7 +604,10 @@
     expert(i)
     first_sum(i)
     to_cross(i).start()
-    lax.fori_loop(0, length // SPAN, spans, 0)
+    lax.fori_loop(0, 2, spans, 0)
+    for t in range(1, min(planes, 3)):
+        forward(t, 0)
+    lax.fori_loop(2, length // SPAN, spans, 0)
     for h in range(heads):
         state_bf[h] = state[h].astype(bf)
     plst[g] = state_bf[...]
@@ -598,14 +616,14 @@
         for copy in in_plane(r):
             copy.start()
     for t in range(1, min(planes, 3)):
-        forward(t)
+        forward(t, 1)
 
     if planes > 1:
+        arrive(1)
+
         @pl.when(early > 0)
         def _():
             arrive(2)
-
-        arrive(1)
     prepare(0)
 
     def turn(u):
@@ -622,7 +640,7 @@
     def pump(u, z):
         @pl.when((u >= 1) & (u < planes - 2))
         def _():
-            forward(u + 2)
+            forward(u + 2, 1)
 
         @pl.when(u == 1)
         def _():
@@ -645,6 +663,12 @@
                 s, r, k = place(c)
                 to_cross(k).start()
 
+        if planes > 1:
+
+            @pl.when(u == 0)
+            def _():
+                forward(3, 0)
+
         @pl.when(u == n - 1 - early)
         def _():
             lax.fori_loop(0, PIECES, mix_final, 0)
@@ -665,7 +689,7 @@
 
         if planes > 1:
 
-            @pl.when(u == 4 - 2 * early)
+            @pl.when(u == 3 - early)
             def _():
                 arrive_twin()
 
@@ -740,7 +764,7 @@
         def _():
             over_x(q * group + g).wait_send()
 
-        @pl.when(s <= early)
+        @pl.when(s == 2 * early)
         def _():
             for r in range(1, group):
                 over_x(q * group + (g + r) % group).wait_send()
@@ -933,9 +957,9 @@
                 VMEM((heads, HEAD, HEAD), f32),
                 VMEM((4, length, width), bf),
                 DMA((16,)), DMA((PIECES,)), DMA((PIECES,)),
-                DMA((2, planes)), DMA((planes,)), DMA((2, planes)), DMA((planes,)),
+                DMA((2, planes, 2)), DMA((planes, 2)), DMA((2, planes)), DMA((planes,)),
                 DMA((planes, group)), DMA((n,)), DMA((2, group)), DMA((2, n)),
-                DMA((2, 2)), DMA((2, 2)), DMA((group,)), DMA((n,)),
+                DMA((2, 3)), DMA((2, 3)), DMA((group,)), DMA((n,)),
                 DMA((planes, group)), DMA((n,)),
             ]
             + [DMA((n,))] * 14

time: 112 us -> 111 us (level)
  the two profiles are of different devices: /device:TPU:0 before, /device:TPU:9 now
where the time goes in v5:
time: 111 us
  Pallas kernels  107 us (96%)
  local copies, waits for them, and re-layouts  3.12 us (3%)
    pallas_call x1, Pallas kernels, shards(): pl.pallas_call(functools.partial(kernel, n, planes, capacity, experts), n...  107 us
    unnamed x4, local copies, waits for them, and re-layouts  3.12 us

profile of v5, /device:TPU:9, one launch (start us, length us, event | category | flops | bytes accessed | tf_op | source)
XLA Modules:
  0.0 110.8 jit_solution(15266879832990749737)
XLA Ops:
  0.6 107.0 %fused.1 = (bf16[1024,512]{1,0:T(8,128)(2,1)}, bf16[128,2048]{1,0:T(8,128)(2,1)}) custom-call(s32[2,512]{1,0:T(2,128)} %bitcast.18, f32[2,512]{1,0:T(2,128)} %bitcast.19, f32[1,256]{1,0:T(1,128)} %bitcast.20, f32[2,1024]{1,0:T(2,128)} %bitcast.15, f32[1,256]{1,0:T(1,128)} %bitcast.21, f32[1,2048]{1,0:T(1,128)} %bitcast.16, f32[1,2048]{1,0:T(1,128)} %bitcast.17, ...), custom_call_target="tpu_custom_call" | custom-call | tf_op jit(solution)/shard_map/fused/pallas_call | solution.py:899
  107.7 0.0 copy-start
  107.7 2.3 %copy.20 = bf16[1024,512]{1,0:T(8,128)(2,1)} copy(bf16[1024,512]{1,0:T(8,128)(2,1)} %get-tuple-element.4) | data formatting | bytes 2097152
  110.0 0.0 copy-done
  110.0 0.8 copy.21
Async XLA Ops:
  107.7 2.3 %copy-start = (bf16[128,2048]{1,0:T(8,128)(2,1)S(1)}, bf16[128,2048]{1,0:T(8,128)(2,1)}, u32[]{:S(2)}) copy-start(bf16[128,2048]{1,0:T(8,128)(2,1)} %get-tuple-element.5) | copy-start | bytes 1572868
